TPU v7x, 32 devices: a whole 2x2x4 slice. The times are simulated.
32 devices in a mesh: sp: 8 (over z, x), tp: 4 (over y, core).
Axes of the slice: x: 2, y: 2, z: 4, core: 2. Of those that a mesh axis runs over, the one named last changes fastest.
Arguments:
- residual: bfloat16 [3072, 2048], P(('sp', 'tp')), may hold values from -6 to 6
- queries: bfloat16 [3072, 1024], P('sp', 'tp'), may hold values from -2.5 to 2.5
- keys: bfloat16 [3072, 256], P('sp', 'tp'), may hold values from -2.5 to 2.5
- values: bfloat16 [3072, 256], P('sp', 'tp'), may hold values from -6 to 6
- documents: int32 [3072], P('sp'), may hold values from 0 to 4, never falling along the last dimension, each value on 1 to 1536 neighbouring positions
- sink: float32 [16], P('tp'), may hold values from 3 to 7
- out_weight: bfloat16 [1024, 2048], replicated, may hold values from -0.1875 to 0.1875
- mix_gain: float32 [2048], replicated, may hold values from 0.1 to 1.9
- ffn_gain: float32 [2048], replicated, may hold values from 0.1 to 1.9
- out_gain: float32 [2048], replicated, may hold values from 0.1 to 1.9
- routes: int32 [3072, 4], P(('sp', 'tp')), may hold values from 0 to 7, all different within a row; in each aligned block of 96 rows (0 to 95, 96 to 191, ...) at most 64 rows name the same one
- route_logits: float32 [3072, 4], P(('sp', 'tp')), may hold values from -4 to 4
- gate_weight: bfloat16 [8, 2048, 2048], P('sp', None, 'tp'), may hold values from -1.41421356 to 1.41421356
- up_weight: bfloat16 [8, 2048, 2048], P('sp', None, 'tp'), may hold values from -1.41421356 to 1.41421356
- down_weight: bfloat16 [8, 2048, 2048], P('sp', 'tp'), may hold values from -0.125 to 0.125
Outputs:
- mixed: bfloat16 [3072, 2048], P(('sp', 'tp'))
Inputs may be any that keep to these rules, and one draw needn't show every extreme that they name: `routes`: each row names 4 different experts. In each aligned block of rows held by one device, no expert is named by more than 64 rows, a bound that some block reaches. `documents`: document numbers never fall along the positions; each document has 1 to 1536 positions, and one has exactly 1536.
All inputs are finite; a program needn't handle non-finite values.
Results may differ from a plain program's by a relative error of at most 0.017.
Values may be sent and summed in bfloat16 or wider, within the bound.
A program may use at most 128 MiB of HBM per device.

v0:
```python
import jax
import jax.numpy as jnp
from jax import lax
from jax.sharding import PartitionSpec as P

HD = 64
TOPK = 4
W = 128


def extended(block, sides, width):
    for axis, dim in sides:
        count = lax.axis_size(axis)
        forward = [(i, i + 1) for i in range(count - 1)]
        backward = [(target, source) for source, target in forward]
        low = lax.ppermute(
            lax.slice_in_dim(block, block.shape[dim] - width, None, axis=dim), axis, forward
        )
        high = lax.ppermute(lax.slice_in_dim(block, 0, width, axis=dim), axis, backward)
        block = jnp.concatenate([low, block, high], axis=dim)
    return block


def turn_heads(block, positions, head_count):
    total = block.shape[0]
    heads = block.astype(jnp.float32).reshape(total, head_count, HD)
    half_size = HD // 2
    inverse = 10000.0 ** (-jnp.arange(half_size, dtype=jnp.float32) / half_size)
    angles = positions.astype(jnp.float32)[:, None] * inverse[None, :]
    cosine = jnp.cos(angles)[:, None, :]
    sine = jnp.sin(angles)[:, None, :]
    first_half = heads[..., :half_size]
    second_half = heads[..., half_size:]
    turned = jnp.concatenate(
        [first_half * cosine - second_half * sine, second_half * cosine + first_half * sine],
        axis=-1,
    )
    return turned.reshape(total, head_count * HD).astype(jnp.bfloat16)


def rms_scale(vector):
    return vector * lax.rsqrt(jnp.mean(vector * vector, axis=-1, keepdims=True) + 1e-06)


def windows(padded_rows, blocks):
    tiled = padded_rows.reshape((blocks + 2, W) + padded_rows.shape[1:])
    return jnp.concatenate([tiled[:-2], tiled[1:-1], tiled[2:]], axis=1)


def assign_slots(route_rows, expert_count, capacity):
    flat_routes = route_rows.reshape(route_rows.shape[0] * TOPK)
    onehot_hits = (
        flat_routes[:, None] == jnp.arange(expert_count, dtype=jnp.int32)[None, :]
    ).astype(jnp.int32)
    slot_number = jnp.sum(jnp.cumsum(onehot_hits, axis=0) * onehot_hits, axis=1) - 1
    return flat_routes * capacity + slot_number


def body(
    residual,
    queries,
    keys,
    values,
    documents,
    sink,
    out_weight,
    mix_gain,
    ffn_gain,
    out_gain,
    routes,
    route_logits,
    gate_weight,
    up_weight,
    down_weight,
):
    tok_rows = queries.shape[0]
    head_count = queries.shape[1] // HD
    kv_count = keys.shape[1] // HD
    group_size = head_count // kv_count
    sp_count = lax.axis_size("sp")
    tp_count = lax.axis_size("tp")
    offset = lax.axis_index("sp") * tok_rows
    positions = offset + jnp.arange(tok_rows, dtype=jnp.int32)
    q_turned = turn_heads(queries, positions, head_count)
    k_turned = turn_heads(keys, positions, kv_count)
    paired = jnp.concatenate([k_turned, values], axis=1)
    wide_pairs, wide_docs = (
        extended(paired, (("sp", 0),), W),
        extended(documents, (("sp", 0),), W),
    )
    blocks = tok_rows // W
    query_blocks = q_turned.reshape(blocks, W, kv_count, group_size, HD)
    pair_win = windows(wide_pairs, blocks)
    key_win = pair_win[..., : kv_count * HD].reshape(blocks, 3 * W, kv_count, HD)
    value_win = pair_win[..., kv_count * HD :].reshape(blocks, 3 * W, kv_count, HD)
    doc_win = windows(wide_docs, blocks)
    doc_query = documents.reshape(blocks, W)
    block_ids = jnp.arange(blocks, dtype=jnp.int32)[:, None, None]
    query_pos = offset + block_ids * W + jnp.arange(W, dtype=jnp.int32)[None, :, None]
    key_pos = offset + (block_ids - 1) * W + jnp.arange(3 * W, dtype=jnp.int32)[None, None, :]
    keep_mask = (
        (jnp.abs(query_pos - key_pos) <= W) & (key_pos >= 0) & (key_pos < tok_rows * sp_count)
    )
    keep_mask = keep_mask & (doc_query[:, :, None] == doc_win[:, None, :])
    scores = jnp.einsum(
        "nqhgd,nkhd->nhgqk", query_blocks, key_win, preferred_element_type=jnp.float32
    ) * HD ** (-0.5)
    exponent = jnp.where(keep_mask[:, None, None], jnp.exp(scores), 0.0)
    denominator = jnp.sum(exponent, axis=-1, keepdims=True) + jnp.exp(sink).reshape(
        1, kv_count, group_size, 1, 1
    )
    probs = (exponent / denominator).astype(jnp.bfloat16)
    attended = jnp.einsum("nhgqk,nkhd->nqhgd", probs, value_win, preferred_element_type=jnp.float32)
    attended = attended.astype(jnp.bfloat16).reshape(tok_rows, head_count * HD)
    own_rows = tok_rows // tp_count
    all_heads = lax.all_to_all(attended, "tp", split_axis=0, concat_axis=1, tiled=True)
    projected = jnp.dot(all_heads, out_weight, preferred_element_type=jnp.float32)
    after_mix = residual.astype(jnp.float32) + rms_scale(projected) * mix_gain
    normed = (rms_scale(after_mix) * ffn_gain).astype(jnp.bfloat16)
    local_experts = gate_weight.shape[0]
    expert_count = local_experts * sp_count
    capacity = max(2, own_rows * TOPK * 4 // (3 * expert_count))
    slot_index = assign_slots(routes, expert_count, capacity)
    token_of = jnp.arange(own_rows * TOPK, dtype=jnp.int32) // TOPK
    model_width = normed.shape[1]
    filled = jnp.full((expert_count * capacity,), own_rows, jnp.int32).at[slot_index].set(token_of)
    with_zero = jnp.concatenate([normed, jnp.zeros((1, model_width), jnp.bfloat16)], axis=0)
    outgoing = with_zero[filled].reshape(expert_count, capacity, model_width)
    incoming = lax.all_to_all(outgoing, "sp", split_axis=0, concat_axis=1, tiled=True)
    rows_in = lax.all_gather(incoming, "tp", axis=1, tiled=True)
    gate_pre = jnp.einsum("erd,edf->erf", rows_in, gate_weight, preferred_element_type=jnp.float32)
    up_pre = jnp.einsum("erd,edf->erf", rows_in, up_weight, preferred_element_type=jnp.float32)
    gated = jnp.minimum(gate_pre, 7.0)
    upper = jnp.clip(up_pre, -7.0, 7.0)
    hidden = ((upper + 1.0) * gated * jax.nn.sigmoid(1.702 * gated)).astype(jnp.bfloat16)
    terms = jnp.einsum("erf,efd->erd", hidden, down_weight, preferred_element_type=jnp.float32)
    own_terms = lax.psum_scatter(terms.astype(jnp.bfloat16), "tp", scatter_dimension=1, tiled=True)
    returned = lax.all_to_all(own_terms, "sp", split_axis=1, concat_axis=0, tiled=True)
    picked = returned.reshape(expert_count * capacity, model_width)[slot_index]
    picked = picked.reshape(own_rows, TOPK, model_width).astype(jnp.float32)
    exp_logits = jnp.exp(route_logits)
    route_weights = exp_logits / jnp.sum(exp_logits, axis=-1, keepdims=True)
    expert_mix = jnp.einsum("rk,rkd->rd", route_weights, picked)
    return (after_mix + rms_scale(expert_mix) * out_gain).astype(jnp.bfloat16)


def solution(mesh):
    in_specs = (
        P(("sp", "tp"), None),
        P("sp", "tp"),
        P("sp", "tp"),
        P("sp", "tp"),
        P("sp"),
        P("tp"),
        P(),
        P(),
        P(),
        P(),
        P(("sp", "tp"), None),
        P(("sp", "tp"), None),
        P("sp", None, "tp"),
        P("sp", None, "tp"),
        P("sp", "tp", None),
    )
    out_specs = P(("sp", "tp"), None)
    return jax.shard_map(body, mesh=mesh, in_specs=in_specs, out_specs=out_specs, check_vma=False)
```

profile of v0, /device:TPU:18, one launch (start us, length us, event | category | flops | bytes accessed | tf_op | source)
XLA Modules:
  0.0 358.4 jit_solution(7261412982960886923)
XLA Ops:
  6.6 1.0 bitcast_convert_fusion
  8.6 3.4 collective-permute-start
  12.0 2.4 collective-permute-start.1
  14.4 0.8 fusion.62
  15.2 4.3 %collective-permute-start.2 = (s32[128]{0:T(128)S(1)}, s32[128]{0:T(128)S(1)}, u32[]{:S(2)}, u32[]{:S(2)}) collective-permute-start(s32[128]{0:T(128)S(1)} %get-tuple-element.18), channel_id=1, source_target_pairs={{0,4},{4,8},{8,12},{12,16},{16,20},{20,24},{24,28},{1,5},{5,9},{9,... | collective-permute-start | bytes 1544 | tf_op jit(solution)/shard_map/ppermute | solution.py:16
  19.5 1.9 collective-permute-start.3
  21.9 0.8 copy.73
  23.6 1.1 copy.66
  24.8 0.9 reduce-window.6
  26.3 2.9 scatter_custom_fusion
  29.3 0.9 fusion.32
  32.8 1.0 reshape.463
  33.7 3.4 all-to-all-start
  37.2 5.2 %all-to-all-done = bf16[4,96,256]{2,1,0:T(8,128)(2,1)S(1)} async-done(((bf16[4,96,256]{2,1,0:T(8,128)(2,1)}), bf16[4,96,256]{2,1,0:T(8,128)(2,1)S(1)}, u32[]{:S(2)}, u32[]{:S(2)}) %all-to-all-start) | async-done | bytes 196640 | tf_op jit(solution)/shard_map/all_to_all | solution.py:116
  42.4 3.1 multiply_reduce_fusion.1
  46.2 3.3 gather_fusion
  49.6 51.2 %all_to_all.40 = bf16[8,64,2048]{2,1,0:T(8,128)(2,1)} all-to-all(bf16[8,64,2048]{2,1,0:T(8,128)(2,1)} %bitcast.125), channel_id=1, replica_groups=mesh['sp'=8,'tp'=4] {'sp'}, dimensions={0} | all-to-all | bytes 4194304 | tf_op jit(solution)/shard_map/all_to_all | solution.py:129
  100.9 59.5 %all-gather.2.cloned.1.call-done = bf16[1,2048,2048]{2,1,0:T(8,128)(2,1)} async-done(((bf16[1,512,2048]{2,1,0:T(8,128)(2,1)}), bf16[1,2048,2048]{2,1,0:T(8,128)(2,1)}) %all-gather.2.cloned.1.call-update) | async-done | bytes 8388624 | tf_op jit(solution)/shard_map/all_gather | solution.py:130
  160.4 10.4 %fusion = f32[2048,512]{1,0:T(8,128)} fusion(bf16[1,2048,2048]{2,1,0:T(8,128)(2,1)} %all-gather.2.cloned.1.call-done, bf16[1,2048,512]{2,1,0:T(8,128)(2,1)} %param.27), kind=kOutput, calls=%fused_computation.3 | convolution fusion | flops 4294967296 | bytes 14680064 | tf_op jit(solution)/shard_map/erd,edf->erf/dot_general | solution.py:131
  170.9 15.2 %convert_bitcast_fusion = bf16[1,2048,2048]{2,1,0:T(8,128)(2,1)} fusion(bf16[1,512,2048]{2,1,0:T(8,128)(2,1)S(1)} %copy-done, f32[2048,512]{1,0:T(8,128)} %fusion, bf16[1,2048,2048]{2,1,0:T(8,128)(2,1)} %all-gather.2.cloned.1.call-done, bf16[1,2048,512]{2,1,0:T(8,128)(2,1)} %param.28), kind=kOutput, calls=%fused_computation.7 | convolution fusion | flops 8604614656 | bytes 25165824 | tf_op jit(solution)/shard_map/erf,efd->erd/dot_general | solution.py:136
  186.1 71.6 %reduce-scatter.2.cloned.1.call-done = bf16[1,512,2048]{2,1,0:T(8,128)(2,1)} async-done(((bf16[1,2048,2048]{2,1,0:T(8,128)(2,1)}), bf16[1,512,2048]{2,1,0:T(8,128)(2,1)}) %reduce-scatter.2.cloned.1.call-update) | async-done | bytes 2097168 | tf_op jit(solution)/shard_map/reduce_scatter | solution.py:137
  257.6 6.7 %copy.97 = bf16[1,512,2048]{2,0,1:T(2,128)(2,1)} copy(bf16[1,512,2048]{2,1,0:T(8,128)(2,1)} %reduce-scatter.2.cloned.1.call-done) | data formatting | bytes 4194304 | tf_op jit(solution)/shard_map/reduce_scatter | solution.py:137
  264.9 13.2 %reduce.5 = bf16[512,2048]{1,0:T(8,128)(2,1)S(1)} reduce(bf16[512,1,2048]{2,1,0:T(2,128)(2,1)} %bitcast.123, bf16[]{:T(256)} %broadcast.379), dimensions={1}, to_apply=%bitcast.120.reduce_sub_computation | reduce | bytes 4194306
  278.0 3.8 %reshape.468 = bf16[8,2,65536]{2,1,0:T(2,128)(2,1)} reshape(bf16[512,2048]{1,0:T(8,128)(2,1)S(1)} %reduce.5) | data formatting | bytes 4194304
  281.9 6.1 %all-to-all-start.2 = ((bf16[8,2,65536]{2,1,0:T(2,128)(2,1)}), bf16[8,2,65536]{2,1,0:T(2,128)(2,1)S(1)}, u32[]{:S(2)}, u32[]{:S(2)}) async-start(bf16[8,2,65536]{2,1,0:T(2,128)(2,1)} %reshape.468), calls=%async_computation.3 | async-start | bytes 4194304 | tf_op jit(solution)/shard_map/all_to_all | solution.py:138
  288.2 44.6 %all-to-all-done.2 = bf16[8,2,65536]{2,1,0:T(2,128)(2,1)S(1)} async-done(((bf16[8,2,65536]{2,1,0:T(2,128)(2,1)}), bf16[8,2,65536]{2,1,0:T(2,128)(2,1)S(1)}, u32[]{:S(2)}, u32[]{:S(2)}) %all-to-all-start.2) | async-done | bytes 2097184 | tf_op jit(solution)/shard_map/all_to_all | solution.py:138
  332.8 4.4 %reshape.469 = bf16[512,1,2048]{2,1,0:T(2,128)(2,1)} reshape(bf16[8,2,65536]{2,1,0:T(2,128)(2,1)S(1)} %all-to-all-done.2) | data formatting | bytes 4194304
  337.2 3.5 copy.96
  340.7 3.1 gather_fusion.1
  343.8 3.6 %reshape.429 = bf16[96,4,2048]{2,1,0:T(4,128)(2,1)} reshape(bf16[384,2048]{1,0:T(8,128)(2,1)} %gather_fusion.1) | data formatting | bytes 3145728 | tf_op jit(solution)/shard_map/reshape | solution.py:140
  347.5 2.5 fusion.63
  350.3 1.2 fusion.29
  (85 shorter events, 7.4 us)
Async XLA Ops:
  6.5 164.3 %copy-start = (bf16[1,512,2048]{2,1,0:T(8,128)(2,1)S(1)}, bf16[1,512,2048]{2,1,0:T(8,128)(2,1)}, u32[]{:S(2)}) copy-start(bf16[1,512,2048]{2,1,0:T(8,128)(2,1)} %param.29) | copy-start | bytes 6291460
  6.5 23.7 %copy-start.4 = (bf16[384,64]{0,1:T(8,128)(2,1)S(1)}, bf16[384,64]{0,1:T(8,128)(2,1)}, u32[]{:S(2)}) copy-start(bf16[384,64]{0,1:T(8,128)(2,1)} %param.18) | copy-start | bytes 147460
  6.5 22.7 %copy-start.6 = (s32[384]{0:T(512)S(1)}, s32[384]{0:T(512)}, u32[]{:S(2)}) copy-start(s32[384]{0:T(512)} %param.19) | copy-start | bytes 4612
  6.5 19.8 %copy-start.10 = (f32[4]{0:T(128)S(1)}, f32[4]{0:T(128)}, u32[]{:S(2)}) copy-start(f32[4]{0:T(128)} %param.20) | copy-start | bytes 52
  8.6 21.6 %collective-permute-start = (bf16[128,128]{0,1:T(8,128)(2,1)S(1)}, bf16[128,128]{0,1:T(8,128)(2,1)S(1)}, u32[]{:S(2)}, u32[]{:S(2)}) collective-permute-start(bf16[128,128]{0,1:T(8,128)(2,1)S(1)} %get-tuple-element.12), channel_id=1, source_target_pairs={{0,4},{4,8},{8,12},{12,16},{16,20},{20,24},{24,28},{1,5},{5,9},{9,... | collective-permute-start | bytes 98312 | tf_op jit(solution)/shard_map/ppermute | solution.py:16
  12.0 18.2 %collective-permute-start.1 = (bf16[128,128]{0,1:T(8,128)(2,1)S(1)}, bf16[128,128]{0,1:T(8,128)(2,1)S(1)}, u32[]{:S(2)}, u32[]{:S(2)}) collective-permute-start(bf16[128,128]{0,1:T(8,128)(2,1)S(1)} %get-tuple-element.13), channel_id=1, source_target_pairs={{4,0},{8,4},{12,8},{16,12},{20,16},{24,20},{28,24},{5,1},{9,5},{13... | collective-permute-start | bytes 98312 | tf_op jit(solution)/shard_map/ppermute | solution.py:19
  15.2 14.1 %collective-permute-start.2 = (s32[128]{0:T(128)S(1)}, s32[128]{0:T(128)S(1)}, u32[]{:S(2)}, u32[]{:S(2)}) collective-permute-start(s32[128]{0:T(128)S(1)} %get-tuple-element.18), channel_id=1, source_target_pairs={{0,4},{4,8},{8,12},{12,16},{16,20},{20,24},{24,28},{1,5},{5,9},{9,... | collective-permute-start | bytes 1544 | tf_op jit(solution)/shard_map/ppermute | solution.py:16
  19.5 9.7 %collective-permute-start.3 = (s32[128]{0:T(128)S(1)}, s32[128]{0:T(128)S(1)}, u32[]{:S(2)}, u32[]{:S(2)}) collective-permute-start(s32[128]{0:T(128)S(1)} %get-tuple-element.19), channel_id=1, source_target_pairs={{4,0},{8,4},{12,8},{16,12},{20,16},{24,20},{28,24},{5,1},{9,5},{13... | collective-permute-start | bytes 1544 | tf_op jit(solution)/shard_map/ppermute | solution.py:19
  33.7 8.6 %all-to-all-start = ((bf16[4,96,256]{2,1,0:T(8,128)(2,1)}), bf16[4,96,256]{2,1,0:T(8,128)(2,1)S(1)}, u32[]{:S(2)}, u32[]{:S(2)}) async-start(bf16[4,96,256]{2,1,0:T(8,128)(2,1)} %reshape.463), calls=%async_computation | async-start | bytes 393216 | tf_op jit(solution)/shard_map/all_to_all | solution.py:116
  37.1 123.3 %all-gather.2.cloned.1.call-start = ((), (), s32[]{:S(2)}) async-start(), calls=%async_computation.4 | async-start | bytes 10485760 | tf_op jit(solution)/shard_map/all_gather | solution.py:130
  42.4 3.2 copy-start.2
  42.4 3.2 copy-start.5
  42.4 3.5 copy-start.7
  100.9 156.8 %reduce-scatter.2.cloned.1.call-start = ((), (), s32[]{:S(2)}) async-start(), calls=%async_computation.5 | async-start | bytes 10485760 | tf_op jit(solution)/shard_map/reduce_scatter | solution.py:137
  281.9 6.2 %copy-start.9 = (f32[96,4]{0,1:T(4,128)S(1)}, f32[96,4]{0,1:T(4,128)}, u32[]{:S(2)}) copy-start(f32[96,4]{0,1:T(4,128)} %param.26) | copy-start | bytes 4612
  281.9 51.0 %all-to-all-start.2 = ((bf16[8,2,65536]{2,1,0:T(2,128)(2,1)}), bf16[8,2,65536]{2,1,0:T(2,128)(2,1)S(1)}, u32[]{:S(2)}, u32[]{:S(2)}) async-start(bf16[8,2,65536]{2,1,0:T(2,128)(2,1)} %reshape.468), calls=%async_computation.3 | async-start | bytes 4194304 | tf_op jit(solution)/shard_map/all_to_all | solution.py:138
  347.5 2.8 copy-start.3
  347.5 2.8 copy-start.8
  347.5 4.1 %copy-start.1 = (bf16[1,512,2048]{2,1,0:T(8,128)(2,1)S(1)}, bf16[1,512,2048]{2,1,0:T(8,128)(2,1)}, u32[]{:S(2)}) copy-start(bf16[1,512,2048]{2,1,0:T(8,128)(2,1)} %param.29) | copy-start | bytes 6291460
Sparse Core Ops, SparseCore 0:
  101.0 59.4 all-gather.1
  186.2 71.3 reduce-scatter.1
where the time goes:
time: 364 us; the launch traced here: 358 us
  waiting for transfers between devices  181 us (50%)
  blocking collectives  51.2 us (14%)
  local copies, waits for them, and re-layouts  37.4 us (10%)
  matrix products  32.6 us (9%)
  starting transfers between devices  21.7 us (6%)
  other arithmetic  20.6 us (6%)
  between operations  13.8 us (4%)
    reduce_scatter x1, waiting for transfers between devices, body(): lax.psum_scatter(terms.astype(jnp.bfloat16), 'tp', scatter_dimension=1, t...  71.6 us
    all_gather x1, waiting for transfers between devices, body(): rows_in = lax.all_gather(incoming, 'tp', axis=1, tiled=True)  59.5 us
    all_to_all x1, blocking collectives, body(): lax.all_to_all(outgoing, 'sp', split_axis=0, concat_axis=1, tiled=True)  51.2 us
    all_to_all x1, waiting for transfers between devices, body(): lax.all_to_all(own_terms, 'sp', split_axis=1, concat_axis=0, tiled=True)  44.6 us
    dot_general x1, matrix products, body(): jnp.einsum('erf,efd->erd', hidden, down_weight, preferred_element_type=jn...  15.2 us
    unnamed x28, local copies, waits for them, and re-layouts  14.1 us
    unnamed x1, other arithmetic  13.2 us
    dot_general x1, matrix products, body(): jnp.einsum('erd,edf->erf', rows_in, gate_weight, preferred_element_type=j...  10.4 us
  transfers between devices with their start and end apart: 8, of which 4 were waited for; matrix products, arithmetic and copies ran while one was open for 3% of the time, Pallas kernels for 0%

commit v1 on v0

--- a/solution.py
+++ b/solution.py
@@ -1,6 +1,10 @@
+import functools
+
 import jax
 import jax.numpy as jnp
 from jax import lax
+from jax.experimental import pallas as pl
+from jax.experimental.pallas import tpu as pltpu
 from jax.sharding import PartitionSpec as P
 
 HD = 64
@@ -47,13 +51,234 @@
     return jnp.concatenate([tiled[:-2], tiled[1:-1], tiled[2:]], axis=1)
 
 
-def assign_slots(route_rows, expert_count, capacity):
-    flat_routes = route_rows.reshape(route_rows.shape[0] * TOPK)
-    onehot_hits = (
-        flat_routes[:, None] == jnp.arange(expert_count, dtype=jnp.int32)[None, :]
-    ).astype(jnp.int32)
-    slot_number = jnp.sum(jnp.cumsum(onehot_hits, axis=0) * onehot_hits, axis=1) - 1
-    return flat_routes * capacity + slot_number
+def flipped(index, bits, size):
+    result, unit = 0, 1
+    while unit < size:
+        result = result + ((index // unit + bits // unit) % 2) * unit
+        unit *= 2
+    return result
+
+
+def expert_kernel(
+    sp_count, tp_count, capacity,
+    outgoing, gate_hbm, up_hbm, down_hbm,
+    returned,
+    gate, up, down, rows, part, core_in, y_out, y_in, done_out,
+    weight_sem, local_sem, send_sem, recv_sem,
+):
+    me = lax.axis_index("sp")
+    tp = lax.axis_index("tp")
+    mate = flipped(tp, 1, tp_count)
+    across = flipped(tp, 2, tp_count)
+    SP, ACROSS, NEAR, NEAR2, CORE, BACK, HOME = range(7)
+
+    def remote(kind, step, source, target, device):
+        return pltpu.make_async_remote_copy(
+            src_ref=source,
+            dst_ref=target,
+            send_sem=send_sem.at[kind, step],
+            recv_sem=recv_sem.at[kind, step],
+            device_id=device,
+            device_id_type=pl.DeviceIdType.MESH,
+        )
+
+    def out_copy(step):
+        peer = flipped(me, step, sp_count)
+        return remote(SP, step, outgoing.at[peer], rows.at[step, 0], {"sp": peer})
+
+    def across_copy(step):
+        return remote(ACROSS, step, rows.at[step, 0], rows.at[step, 1], {"tp": across})
+
+    def near_copy(step):
+        return remote(NEAR, step, rows.at[step, 0], rows.at[step, 2], {"tp": mate})
+
+    def near2_copy(step):
+        return remote(NEAR2, step, rows.at[step, 1], rows.at[step, 3], {"tp": mate})
+
+    def core_copy(step):
+        return remote(CORE, step, part.at[step, pl.ds(2, 2)], core_in.at[step], {"tp": mate})
+
+    def back_copy(step):
+        return remote(BACK, step, y_out.at[step], y_in.at[step], {"tp": across})
+
+    def home_copy(step):
+        peer = flipped(me, step, sp_count)
+        return remote(HOME, step, done_out.at[step], returned.at[me], {"sp": peer})
+
+    weights = [
+        pltpu.make_async_copy(source, target, weight_sem.at[n])
+        for n, (source, target) in enumerate(((gate_hbm, gate), (up_hbm, up), (down_hbm, down)))
+    ]
+    own_in = pltpu.make_async_copy(outgoing.at[me], rows.at[0, 0], local_sem.at[0])
+    own_out = pltpu.make_async_copy(done_out.at[0], returned.at[me], local_sem.at[1])
+
+    barrier = pltpu.get_barrier_semaphore()
+    own_in.start()
+
+    def greet(step, carry):
+        pl.semaphore_signal(
+            barrier, inc=1, device_id={"sp": flipped(me, step, sp_count)},
+            device_id_type=pl.DeviceIdType.MESH,
+        )
+        return carry
+
+    lax.fori_loop(1, sp_count, greet, 0)
+    for near in (mate, across):
+        pl.semaphore_signal(
+            barrier, inc=1, device_id={"tp": near}, device_id_type=pl.DeviceIdType.MESH
+        )
+    pl.semaphore_wait(barrier, sp_count + 1)
+
+    def send_out(step, carry):
+        out_copy(step).start()
+        return carry
+
+    lax.fori_loop(1, sp_count, send_out, 0)
+    for copy in weights:
+        copy.start()
+    own_in.wait()
+
+    local_experts, width, units = gate.shape
+    slots = rows.shape[2]
+    chunk = tp_count * slots
+
+    def forward(step):
+        @pl.when(step > 0)
+        def _():
+            out_copy(step).wait_recv()
+
+        across_copy(step).start()
+        near_copy(step).start()
+
+    def forward_again(step):
+        across_copy(step).wait_recv()
+        near2_copy(step).start()
+
+    def compute(step):
+        @pl.when(step == 0)
+        def _():
+            for copy in weights:
+                copy.wait()
+
+        near_copy(step).wait_recv()
+        near2_copy(step).wait_recv()
+        block = rows[step].reshape(chunk, width)
+        hiddens = []
+        for expert in range(local_experts):
+            gate_pre = jnp.dot(block, gate[expert], preferred_element_type=jnp.float32)
+            up_pre = jnp.dot(block, up[expert], preferred_element_type=jnp.float32)
+            gated = jnp.minimum(gate_pre, 7.0)
+            upper = jnp.clip(up_pre, -7.0, 7.0)
+            hidden = (upper + 1.0) * gated * jax.nn.sigmoid(1.702 * gated)
+            if local_experts > 1:
+                row = lax.broadcasted_iota(jnp.int32, (chunk, units), 0)
+                hidden = jnp.where((row // capacity) % local_experts == expert, hidden, 0.0)
+            hiddens.append(hidden.astype(jnp.bfloat16))
+        tile = width // 4
+        for start in range(0, width, tile):
+            total = jnp.dot(
+                hiddens[0], down[0, :, start : start + tile], preferred_element_type=jnp.float32
+            )
+            for expert in range(1, local_experts):
+                total = total + jnp.dot(
+                    hiddens[expert], down[expert, :, start : start + tile],
+                    preferred_element_type=jnp.float32,
+                )
+            part[step, :, :, start : start + tile] = total.astype(jnp.bfloat16).reshape(
+                tp_count, slots, tile
+            )
+        core_copy(step).start()
+
+    def add_core(step):
+        core_copy(step).wait_recv()
+        y_out[step] = (
+            part[step, 1].astype(jnp.float32) + core_in[step, 1].astype(jnp.float32)
+        ).astype(jnp.bfloat16)
+        back_copy(step).start()
+
+    def add_across(step):
+        back_copy(step).wait_recv()
+        done_out[step] = (
+            part[step, 0].astype(jnp.float32)
+            + core_in[step, 0].astype(jnp.float32)
+            + y_in[step].astype(jnp.float32)
+        ).astype(jnp.bfloat16)
+
+        @pl.when(step == 0)
+        def _():
+            own_out.start()
+
+        @pl.when(step > 0)
+        def _():
+            home_copy(step).start()
+
+    stages = ((forward_again, 1), (compute, 2), (add_core, 3), (add_across, 4), (forward, 0))
+
+    def turn(number, carry):
+        for stage, lag in stages:
+            step = number - lag
+
+            @pl.when((step >= 0) & (step < sp_count))
+            def _():
+                stage(step)
+
+        return carry
+
+    lax.fori_loop(0, sp_count + 4, turn, 0)
+
+    def finish(step, carry):
+        @pl.when(step > 0)
+        def _():
+            out_copy(step).wait_send()
+            home_copy(step).wait_send()
+            home_copy(step).wait_recv()
+
+        for make in (across_copy, near_copy, near2_copy, core_copy, back_copy):
+            make(step).wait_send()
+        return carry
+
+    lax.fori_loop(0, sp_count, finish, 0)
+    own_out.wait()
+
+
+def run_experts(outgoing, gate_weight, up_weight, down_weight, capacity):
+    sp_count, slots, width = outgoing.shape
+    tp_count = lax.axis_size("tp")
+    assert tp_count == 4
+    local_experts, _, units = gate_weight.shape
+    rows = sp_count * tp_count * slots
+    half = jnp.bfloat16
+    anywhere = pl.BlockSpec(memory_space=pl.ANY)
+    return pl.pallas_call(
+        functools.partial(expert_kernel, sp_count, tp_count, capacity),
+        out_shape=jax.ShapeDtypeStruct(outgoing.shape, half),
+        in_specs=[anywhere] * 4,
+        out_specs=anywhere,
+        scratch_shapes=[
+            pltpu.VMEM(gate_weight.shape, half),
+            pltpu.VMEM(up_weight.shape, half),
+            pltpu.VMEM(down_weight.shape, half),
+            pltpu.VMEM((sp_count, tp_count, slots, width), half),
+            pltpu.VMEM((sp_count, tp_count, slots, width), half),
+            pltpu.VMEM((sp_count, 2, slots, width), half),
+            pltpu.VMEM((sp_count, slots, width), half),
+            pltpu.VMEM((sp_count, slots, width), half),
+            pltpu.VMEM((sp_count, slots, width), half),
+            pltpu.SemaphoreType.DMA((3,)),
+            pltpu.SemaphoreType.DMA((2,)),
+            pltpu.SemaphoreType.DMA((7, sp_count)),
+            pltpu.SemaphoreType.DMA((7, sp_count)),
+        ],
+        compiler_params=pltpu.CompilerParams(
+            collective_id=0, has_side_effects=True, vmem_limit_bytes=60 * 1024 * 1024
+        ),
+        cost_estimate=pl.CostEstimate(
+            flops=6 * rows * local_experts * width * units,
+            bytes_accessed=6 * local_experts * width * units,
+            transcendentals=rows * units,
+        ),
+        name="experts",
+    )(outgoing, gate_weight, up_weight, down_weight)
 
 
 def body(
@@ -120,27 +345,35 @@
     local_experts = gate_weight.shape[0]
     expert_count = local_experts * sp_count
     capacity = max(2, own_rows * TOPK * 4 // (3 * expert_count))
-    slot_index = assign_slots(routes, expert_count, capacity)
-    token_of = jnp.arange(own_rows * TOPK, dtype=jnp.int32) // TOPK
-    model_width = normed.shape[1]
-    filled = jnp.full((expert_count * capacity,), own_rows, jnp.int32).at[slot_index].set(token_of)
-    with_zero = jnp.concatenate([normed, jnp.zeros((1, model_width), jnp.bfloat16)], axis=0)
-    outgoing = with_zero[filled].reshape(expert_count, capacity, model_width)
-    incoming = lax.all_to_all(outgoing, "sp", split_axis=0, concat_axis=1, tiled=True)
-    rows_in = lax.all_gather(incoming, "tp", axis=1, tiled=True)
-    gate_pre = jnp.einsum("erd,edf->erf", rows_in, gate_weight, preferred_element_type=jnp.float32)
-    up_pre = jnp.einsum("erd,edf->erf", rows_in, up_weight, preferred_element_type=jnp.float32)
-    gated = jnp.minimum(gate_pre, 7.0)
-    upper = jnp.clip(up_pre, -7.0, 7.0)
-    hidden = ((upper + 1.0) * gated * jax.nn.sigmoid(1.702 * gated)).astype(jnp.bfloat16)
-    terms = jnp.einsum("erf,efd->erd", hidden, down_weight, preferred_element_type=jnp.float32)
-    own_terms = lax.psum_scatter(terms.astype(jnp.bfloat16), "tp", scatter_dimension=1, tiled=True)
-    returned = lax.all_to_all(own_terms, "sp", split_axis=1, concat_axis=0, tiled=True)
-    picked = returned.reshape(expert_count * capacity, model_width)[slot_index]
-    picked = picked.reshape(own_rows, TOPK, model_width).astype(jnp.float32)
     exp_logits = jnp.exp(route_logits)
     route_weights = exp_logits / jnp.sum(exp_logits, axis=-1, keepdims=True)
-    expert_mix = jnp.einsum("rk,rkd->rd", route_weights, picked)
+    named = routes[:, :, None] == jnp.arange(expert_count, dtype=jnp.int32)
+    hits = jnp.any(named, axis=1)
+    expert_weights = jnp.sum(jnp.where(named, route_weights[:, :, None], 0.0), axis=1)
+    row_ids = jnp.arange(own_rows, dtype=jnp.int32)
+    lower = (row_ids[:, None] >= row_ids[None, :]).astype(jnp.bfloat16)
+    places = jnp.dot(lower, hits.astype(jnp.bfloat16), preferred_element_type=jnp.float32)
+    places = jnp.where(hits, places.astype(jnp.int32) - 1, -1)
+    slot_ids = jnp.arange(capacity, dtype=jnp.int32)
+    total_slots = expert_count * capacity
+    chosen = places[:, :, None] == slot_ids
+    pick = (places.T[:, None, :] == slot_ids[None, :, None]).reshape(total_slots, own_rows)
+    outgoing = jnp.dot(
+        pick.astype(jnp.bfloat16), normed, preferred_element_type=jnp.float32
+    ).astype(jnp.bfloat16)
+    model_width = normed.shape[1]
+    outgoing = outgoing.reshape(sp_count, local_experts * capacity, model_width)
+    returned = run_experts(outgoing, gate_weight, up_weight, down_weight, capacity)
+    returned = returned.reshape(total_slots, model_width)
+    high = expert_weights.astype(jnp.bfloat16).astype(jnp.float32)
+    low = expert_weights - high
+
+    def spread(weights):
+        wide = jnp.where(chosen, weights[:, :, None], 0.0)
+        return wide.reshape(own_rows, total_slots).astype(jnp.bfloat16)
+
+    expert_mix = jnp.dot(spread(high), returned, preferred_element_type=jnp.float32)
+    expert_mix = expert_mix + jnp.dot(spread(low), returned, preferred_element_type=jnp.float32)
     return (after_mix + rms_scale(expert_mix) * out_gain).astype(jnp.bfloat16)
 
 

time: 364 us -> 178 us (0.49); the launches traced: 358 us -> 177 us
  waiting for transfers between devices: 181 us -> 5.49 us
  Pallas kernels: 0 us -> 135 us
  blocking collectives: 51.2 us -> 0 us
  local copies, waits for them, and re-layouts: 37.4 us -> 4.05 us
  matrix products: 32.6 us -> 9.65 us
  other arithmetic: 20.6 us -> 7.05 us
  between operations: 13.8 us -> 0.38 us
  starting transfers between devices: 21.7 us -> 15.5 us
    pallas_call x0 -> x1, Pallas kernels: none -> 135 us  [run_experts(): pl.pallas_call(functools.partial(expert_kernel, sp_count, tp_count, capac...]
    reduce_scatter x1 -> x0, waiting for transfers between devices: 71.6 us -> none  [body(): lax.psum_scatter(terms.astype(jnp.bfloat16), 'tp', scatter_dimension=1, t...]
    all_gather x1 -> x0, waiting for transfers between devices: 59.5 us -> none  [body(): rows_in = lax.all_gather(incoming, 'tp', axis=1, tiled=True)]
    all_to_all x1 -> x0, blocking collectives: 51.2 us -> none  [body(): lax.all_to_all(outgoing, 'sp', split_axis=0, concat_axis=1, tiled=True)]
    all_to_all x1 -> x0, waiting for transfers between devices: 44.6 us -> none  [body(): lax.all_to_all(own_terms, 'sp', split_axis=1, concat_axis=0, tiled=True)]
    dot_general x3 -> x4, matrix products: 28.1 us -> 5.16 us  [the longest x1 2.24 us: body(): jnp.dot(spread(low), returned, preferred_element_type=jnp.float32)]
    unnamed x1 -> x0, other arithmetic: 13.2 us -> none
    unnamed x28 -> x19, local copies, waits for them, and re-layouts: 14.1 us -> 1.22 us
  transfers between devices with their start and end apart: 8 -> 5, of which waited for: 4 -> 2; matrix products, arithmetic and copies ran while one was open for 3% -> 3% of each run, Pallas kernels for 0% -> 0%
where the time goes in v1:
time: 178 us; the launch traced here: 177 us
  Pallas kernels  135 us (76%)
  starting transfers between devices  15.5 us (9%)
  matrix products  9.65 us (5%)
  other arithmetic  7.05 us (4%)
  waiting for transfers between devices  5.49 us (3%)
  local copies, waits for them, and re-layouts  4.05 us (2%)
    pallas_call x1, Pallas kernels, run_experts(): pl.pallas_call(functools.partial(expert_kernel, sp_count, tp_count, capac...  135 us
    ppermute x2, starting transfers between devices, extended(): lax.ppermute(lax.slice_in_dim(block, block.shape[dim] - width, None, axis...  7.79 us
    all_to_all x1, waiting for transfers between devices, body(): lax.all_to_all(attended, 'tp', split_axis=0, concat_axis=1, tiled=True)  5.26 us
    ppermute x2, starting transfers between devices, extended(): lax.ppermute(lax.slice_in_dim(block, 0, width, axis=dim), axis, backward)  4.31 us
  transfers between devices with their start and end apart: 5, of which 2 were waited for; matrix products, arithmetic and copies ran while one was open for 3% of the time, Pallas kernels for 0%

profile of v1, /device:TPU:18, one launch (start us, length us, event | category | flops | bytes accessed | tf_op | source)
XLA Modules:
  0.0 177.3 jit_solution(14990674818785509372)
XLA Ops:
  0.1 0.8 bitcast_convert_fusion
  0.9 0.3 fusion.31
  1.1 0.7 fusion.34
  1.9 3.4 %collective-permute-start = (bf16[128,128]{0,1:T(8,128)(2,1)S(1)}, bf16[128,128]{0,1:T(8,128)(2,1)S(1)}, u32[]{:S(2)}, u32[]{:S(2)}) collective-permute-start(bf16[128,128]{0,1:T(8,128)(2,1)S(1)} %get-tuple-element.12), channel_id=1, source_target_pairs={{0,4},{4,8},{8,12},{12,16},{16,20},{20,24},{24,28},{1,5},{5,9},{9,... | collective-permute-start | bytes 98312 | tf_op jit(solution)/shard_map/ppermute | solution.py:20
  5.3 2.4 %collective-permute-start.1 = (bf16[128,128]{0,1:T(8,128)(2,1)S(1)}, bf16[128,128]{0,1:T(8,128)(2,1)S(1)}, u32[]{:S(2)}, u32[]{:S(2)}) collective-permute-start(bf16[128,128]{0,1:T(8,128)(2,1)S(1)} %get-tuple-element.13), channel_id=1, source_target_pairs={{4,0},{8,4},{12,8},{16,12},{20,16},{24,20},{28,24},{5,1},{9,5},{13... | collective-permute-start | bytes 98312 | tf_op jit(solution)/shard_map/ppermute | solution.py:23
  7.7 0.8 fusion.44
  8.5 4.3 %collective-permute-start.2 = (s32[128]{0:T(128)S(1)}, s32[128]{0:T(128)S(1)}, u32[]{:S(2)}, u32[]{:S(2)}) collective-permute-start(s32[128]{0:T(128)S(1)} %get-tuple-element.18), channel_id=1, source_target_pairs={{0,4},{4,8},{8,12},{12,16},{16,20},{20,24},{24,28},{1,5},{5,9},{9,... | collective-permute-start | bytes 1544 | tf_op jit(solution)/shard_map/ppermute | solution.py:20
  12.9 1.9 %collective-permute-start.3 = (s32[128]{0:T(128)S(1)}, s32[128]{0:T(128)S(1)}, u32[]{:S(2)}, u32[]{:S(2)}) collective-permute-start(s32[128]{0:T(128)S(1)} %get-tuple-element.19), channel_id=1, source_target_pairs={{4,0},{8,4},{12,8},{16,12},{20,16},{24,20},{28,24},{5,1},{9,5},{13... | collective-permute-start | bytes 1544 | tf_op jit(solution)/shard_map/ppermute | solution.py:23
  14.9 0.3 multiply_cosine_fusion
  15.3 1.1 copy.61
  16.4 0.7 fusion.36
  17.1 0.1 fusion.11
  17.2 0.7 exponential_reduce_fusion
  17.9 0.7 exponential_divide_fusion
  18.8 0.1 bitcast_compare_fusion
  19.0 0.2 collective-permute-done.3
  19.3 0.9 fusion.14
  20.6 0.1 copy.59
  20.8 0.1 copy.60
  21.0 0.7 fusion.1
  21.8 0.7 fusion.7
  22.5 0.3 copy.70
  22.7 1.0 reshape.372
  23.7 3.4 %all-to-all-start = ((bf16[4,96,256]{2,1,0:T(8,128)(2,1)}), bf16[4,96,256]{2,1,0:T(8,128)(2,1)S(1)}, u32[]{:S(2)}, u32[]{:S(2)}) async-start(bf16[4,96,256]{2,1,0:T(8,128)(2,1)} %reshape.372), calls=%async_computation | async-start | bytes 393216 | tf_op jit(solution)/shard_map/all_to_all | solution.py:341
  27.1 5.3 %all-to-all-done = bf16[4,96,256]{2,1,0:T(8,128)(2,1)S(1)} async-done(((bf16[4,96,256]{2,1,0:T(8,128)(2,1)}), bf16[4,96,256]{2,1,0:T(8,128)(2,1)S(1)}, u32[]{:S(2)}, u32[]{:S(2)}) %all-to-all-start) | async-done | bytes 196640 | tf_op jit(solution)/shard_map/all_to_all | solution.py:341
  32.4 3.1 %multiply_reduce_fusion.2 = (f32[96]{0:T(128)S(1)}, f32[96,2048]{1,0:T(8,128)S(1)}) fusion(bf16[96,1024]{1,0:T(8,128)(2,1)S(1)} %bitcast.86, bf16[1024,2048]{1,0:T(8,128)(2,1)} %param.21), kind=kOutput, calls=%fused_computation.19 | convolution fusion | flops 403046304 | bytes 5177728 | tf_op jit(solution)/shard_map/dot_general | solution.py:342
  35.6 0.3 multiply_reduce_fusion.1
  35.9 2.2 %convolution_convert_fusion = bf16[512,2048]{1,0:T(8,128)(2,1)} fusion(pred[512,96]{1,0:T(32,128)(4,1)S(1)} %bitcast_compare_fusion, f32[2048]{0:T(1024)S(1)} %copy-done.5, f32[96]{0:T(128)S(1)} %add_rsqrt_fusion.1, f32[96,2048]{1,0:T(8,128)S(1)} %get-tuple-element.25, bf16[96,2048]{1,0:T(8,128)(2,1)S(1)} %copy-done.1, f32[2048]{0:T(1024)S(1)} %copy-done.3, ...), kind=kOutput, calls=%fused_computation | convolution fusion | flops 203751424 | bytes 3343104 | tf_op jit(solution)/shard_map/dot_general | solution.py:361
  38.1 135.2 %experts.1 = bf16[8,64,2048]{2,1,0:T(8,128)(2,1)} custom-call(bf16[8,64,2048]{2,1,0:T(8,128)(2,1)} %bitcast.83, bf16[1,2048,512]{2,1,0:T(8,128)(2,1)} %gate_hbm.1, bf16[1,2048,512]{2,1,0:T(8,128)(2,1)} %up_hbm.1, bf16[1,512,2048]{2,1,0:T(8,128)(2,1)} %down_hbm.1), custom_call_target="tpu_custom_call" | custom-call | flops 12884901888 | bytes 6291456 | tf_op jit(solution)/shard_map/experts/pallas_call | solution.py:252
  173.3 2.2 %convolution_bitcast_fusion = f32[96,2048]{1,0:T(8,128)S(1)} fusion(bf16[8,64,2048]{2,1,0:T(8,128)(2,1)} %experts.1, bf16[96,8]{0,1:T(8,128)(2,1)S(1)} %fusion.39, s32[96,8]{0,1:T(8,128)S(1)} %fusion.11), kind=kOutput, calls=%fused_computation.1 | convolution fusion | flops 201424896 | bytes 2888192 | tf_op jit(solution)/shard_map/dot_general | solution.py:376
  175.6 0.6 multiply_reduce_fusion
  176.3 1.0 add_convert_fusion
  (50 shorter events, 1.3 us)
Async XLA Ops:
  0.0 20.1 %copy-start.2 = (bf16[384,64]{0,1:T(8,128)(2,1)S(1)}, bf16[384,64]{0,1:T(8,128)(2,1)}, u32[]{:S(2)}) copy-start(bf16[384,64]{0,1:T(8,128)(2,1)} %param.18) | copy-start | bytes 147460
  0.0 19.2 %copy-start.4 = (s32[384]{0:T(512)S(1)}, s32[384]{0:T(512)}, u32[]{:S(2)}) copy-start(s32[384]{0:T(512)} %param.19) | copy-start | bytes 4612
  0.0 18.7 %copy-start.7 = (s32[96,4]{0,1:T(4,128)S(1)}, s32[96,4]{0,1:T(4,128)}, u32[]{:S(2)}) copy-start(s32[96,4]{0,1:T(4,128)} %param.25) | copy-start | bytes 4612
  0.0 18.7 %copy-start.8 = (f32[4]{0:T(128)S(1)}, f32[4]{0:T(128)}, u32[]{:S(2)}) copy-start(f32[4]{0:T(128)} %param.20) | copy-start | bytes 52
  1.9 18.2 %collective-permute-start = (bf16[128,128]{0,1:T(8,128)(2,1)S(1)}, bf16[128,128]{0,1:T(8,128)(2,1)S(1)}, u32[]{:S(2)}, u32[]{:S(2)}) collective-permute-start(bf16[128,128]{0,1:T(8,128)(2,1)S(1)} %get-tuple-element.12), channel_id=1, source_target_pairs={{0,4},{4,8},{8,12},{12,16},{16,20},{20,24},{24,28},{1,5},{5,9},{9,... | collective-permute-start | bytes 98312 | tf_op jit(solution)/shard_map/ppermute | solution.py:20
  5.3 14.8 %collective-permute-start.1 = (bf16[128,128]{0,1:T(8,128)(2,1)S(1)}, bf16[128,128]{0,1:T(8,128)(2,1)S(1)}, u32[]{:S(2)}, u32[]{:S(2)}) collective-permute-start(bf16[128,128]{0,1:T(8,128)(2,1)S(1)} %get-tuple-element.13), channel_id=1, source_target_pairs={{4,0},{8,4},{12,8},{16,12},{20,16},{24,20},{28,24},{5,1},{9,5},{13... | collective-permute-start | bytes 98312 | tf_op jit(solution)/shard_map/ppermute | solution.py:23
  8.5 10.5 %collective-permute-start.2 = (s32[128]{0:T(128)S(1)}, s32[128]{0:T(128)S(1)}, u32[]{:S(2)}, u32[]{:S(2)}) collective-permute-start(s32[128]{0:T(128)S(1)} %get-tuple-element.18), channel_id=1, source_target_pairs={{0,4},{4,8},{8,12},{12,16},{16,20},{20,24},{24,28},{1,5},{5,9},{9,... | collective-permute-start | bytes 1544 | tf_op jit(solution)/shard_map/ppermute | solution.py:20
  12.9 6.4 %collective-permute-start.3 = (s32[128]{0:T(128)S(1)}, s32[128]{0:T(128)S(1)}, u32[]{:S(2)}, u32[]{:S(2)}) collective-permute-start(s32[128]{0:T(128)S(1)} %get-tuple-element.19), channel_id=1, source_target_pairs={{4,0},{8,4},{12,8},{16,12},{20,16},{24,20},{28,24},{5,1},{9,5},{13... | collective-permute-start | bytes 1544 | tf_op jit(solution)/shard_map/ppermute | solution.py:23
  23.7 8.6 %all-to-all-start = ((bf16[4,96,256]{2,1,0:T(8,128)(2,1)}), bf16[4,96,256]{2,1,0:T(8,128)(2,1)S(1)}, u32[]{:S(2)}, u32[]{:S(2)}) async-start(bf16[4,96,256]{2,1,0:T(8,128)(2,1)} %reshape.372), calls=%async_computation | async-start | bytes 393216 | tf_op jit(solution)/shard_map/all_to_all | solution.py:341
  32.3 3.2 %copy-start.1 = (bf16[96,2048]{1,0:T(8,128)(2,1)S(1)}, bf16[96,2048]{1,0:T(8,128)(2,1)}, u32[]{:S(2)}) copy-start(bf16[96,2048]{1,0:T(8,128)(2,1)} %param.15) | copy-start | bytes 1179652
  32.4 3.2 %copy-start.3 = (f32[2048]{0:T(1024)S(1)}, f32[2048]{0:T(1024)}, u32[]{:S(2)}) copy-start(f32[2048]{0:T(1024)} %param.22) | copy-start | bytes 24580
  32.4 3.5 %copy-start.5 = (f32[2048]{0:T(1024)S(1)}, f32[2048]{0:T(1024)}, u32[]{:S(2)}) copy-start(f32[2048]{0:T(1024)} %param.23) | copy-start | bytes 24580
  173.3 2.3 %copy-start = (bf16[8,64,2048]{2,1,0:T(8,128)(2,1)S(1)}, bf16[8,64,2048]{2,1,0:T(8,128)(2,1)}, u32[]{:S(2)}) copy-start(bf16[8,64,2048]{2,1,0:T(8,128)(2,1)} %experts.1) | copy-start | bytes 6291460
  175.6 0.7 copy-start.6

commit v2 on v1

--- a/solution.py
+++ b/solution.py
@@ -12,43 +12,187 @@
 W = 128
 
 
-def extended(block, sides, width):
-    for axis, dim in sides:
-        count = lax.axis_size(axis)
-        forward = [(i, i + 1) for i in range(count - 1)]
-        backward = [(target, source) for source, target in forward]
-        low = lax.ppermute(
-            lax.slice_in_dim(block, block.shape[dim] - width, None, axis=dim), axis, forward
-        )
-        high = lax.ppermute(lax.slice_in_dim(block, 0, width, axis=dim), axis, backward)
-        block = jnp.concatenate([low, block, high], axis=dim)
-    return block
-
-
-def turn_heads(block, positions, head_count):
-    total = block.shape[0]
-    heads = block.astype(jnp.float32).reshape(total, head_count, HD)
+def rms_scale(vector):
+    return vector * lax.rsqrt(jnp.mean(vector * vector, axis=-1, keepdims=True) + 1e-06)
+
+
+def attention_kernel(
+    sp_count, tp_count,
+    queries, keys, values, documents, doc_column, cosine, sine, sink_terms,
+    heads_out,
+    wide_keys, wide_values, wide_docs, turned_keys, attended,
+    local_sem, send_sem, recv_sem, out_send, out_recv,
+):
+    me = lax.axis_index("sp")
+    tp = lax.axis_index("tp")
+    right = (me + 1) % sp_count
+    left = (me + sp_count - 1) % sp_count
+    tok_rows, width = queries.shape
+    blocks = tok_rows // W
+    kv_count = keys.shape[1] // HD
+    group_size = width // HD // kv_count
+    own_rows = tok_rows // tp_count
+    total = tok_rows * sp_count
+    mesh_id = pl.DeviceIdType.MESH
+
+    inside = pl.ds(W, tok_rows)
+    locals_in = [
+        pltpu.make_async_copy(source, target, local_sem.at[n])
+        for n, (source, target) in enumerate(
+            (
+                (keys, wide_keys.at[inside]),
+                (values, wide_values.at[inside]),
+                (documents, wide_docs.at[pl.ds(1, blocks)]),
+            )
+        )
+    ]
+    for copy in locals_in:
+        copy.start()
+
+    barrier = pltpu.get_barrier_semaphore()
+    for neighbour in (left, right):
+        pl.semaphore_signal(barrier, inc=1, device_id={"sp": neighbour}, device_id_type=mesh_id)
+    for hop in range(1, tp_count):
+        pl.semaphore_signal(
+            barrier, inc=1, device_id={"tp": (tp + hop) % tp_count}, device_id_type=mesh_id
+        )
+    pl.semaphore_wait(barrier, 2 + tp_count - 1)
+
+    low, high = pl.ds(0, W), pl.ds(tok_rows + W, W)
+    last = pl.ds(tok_rows - W, W)
+    pairs = (
+        (keys.at[last], wide_keys.at[low], right),
+        (values.at[last], wide_values.at[low], right),
+        (documents.at[blocks - 1], wide_docs.at[0], right),
+        (keys.at[low], wide_keys.at[high], left),
+        (values.at[low], wide_values.at[high], left),
+        (documents.at[0], wide_docs.at[blocks + 1], left),
+    )
+    halos = [
+        pltpu.make_async_remote_copy(
+            src_ref=source, dst_ref=target, send_sem=send_sem.at[n], recv_sem=recv_sem.at[n],
+            device_id={"sp": device}, device_id_type=mesh_id,
+        )
+        for n, (source, target, device) in enumerate(pairs)
+    ]
+    for copy in halos:
+        copy.start()
+
+    def turn(block, rows):
+        size = block.shape[1]
+        wide = block.astype(jnp.float32)
+        lane = lax.broadcasted_iota(jnp.int32, block.shape, 1)
+        swapped = jnp.where(
+            lane % HD < HD // 2, jnp.roll(wide, -(HD // 2), 1), jnp.roll(wide, HD // 2, 1)
+        )
+        copies = size // HD
+        cos = jnp.concatenate([cosine[rows, :]] * copies, axis=1)
+        sin = jnp.concatenate([sine[rows, :]] * copies, axis=1)
+        return (wide * cos + swapped * sin).astype(jnp.bfloat16)
+
+    turned_queries = [
+        turn(queries[n * W : (n + 1) * W, :], slice((n + 1) * W, (n + 2) * W))
+        for n in range(blocks)
+    ]
+    for copy in locals_in:
+        copy.wait()
+    for copy in halos:
+        copy.wait()
+    for n in range(blocks + 2):
+        rows = slice(n * W, (n + 1) * W)
+        turned_keys[rows, :] = turn(wide_keys[rows, :], rows)
+
+    scale = HD ** (-0.5)
+    for n in range(blocks):
+        start = me * tok_rows + n * W
+        query_pos = lax.broadcasted_iota(jnp.int32, (W, 3 * W), 0) + W
+        key_pos = lax.broadcasted_iota(jnp.int32, (W, 3 * W), 1)
+        place = key_pos + (start - W)
+        doc_keys = jnp.concatenate([wide_docs[n + m] for m in range(3)], axis=1)
+        keep = (jnp.abs(query_pos - key_pos) <= W) & (place >= 0) & (place < total)
+        keep = keep & (doc_column[n * W : (n + 1) * W, :] == doc_keys)
+        for head in range(kv_count * group_size):
+            kv = slice(head // group_size * HD, (head // group_size + 1) * HD)
+            columns = slice(head * HD, (head + 1) * HD)
+            window = slice(n * W, (n + 3) * W)
+            scores = lax.dot_general(
+                turned_queries[n][:, columns], turned_keys[window, kv],
+                (((1,), (1,)), ((), ())), preferred_element_type=jnp.float32,
+            ) * scale
+            exponent = jnp.where(keep, jnp.exp(scores), 0.0)
+            denominator = jnp.sum(exponent, axis=-1, keepdims=True) + sink_terms[head]
+            probs = (exponent / denominator).astype(jnp.bfloat16)
+            found = jnp.dot(probs, wide_values[window, kv], preferred_element_type=jnp.float32)
+            attended[n * W : (n + 1) * W, columns] = found.astype(jnp.bfloat16)
+
+    def share(index):
+        return attended.at[pl.ds(pl.multiple_of(index * own_rows, own_rows), own_rows)]
+
+    mine = heads_out.at[:, pl.ds(pl.multiple_of(tp * width, width), width)]
+    sends = []
+    for hop in range(1, tp_count):
+        peer = (tp + hop) % tp_count
+        sends.append(
+            pltpu.make_async_remote_copy(
+                src_ref=share(peer), dst_ref=mine, send_sem=out_send.at[hop],
+                recv_sem=out_recv.at[hop], device_id={"tp": peer}, device_id_type=mesh_id,
+            )
+        )
+    for copy in sends:
+        copy.start()
+    own = pltpu.make_async_copy(share(tp), mine, local_sem.at[3])
+    own.start()
+    own.wait()
+    for copy in sends:
+        copy.wait()
+
+
+def run_attention(queries, keys, values, documents, sink):
+    sp_count = lax.axis_size("sp")
+    tp_count = lax.axis_size("tp")
+    tok_rows, width = queries.shape
+    blocks = tok_rows // W
     half_size = HD // 2
+    first = lax.axis_index("sp") * tok_rows - W
+    positions = first + jnp.arange(tok_rows + 2 * W, dtype=jnp.int32)
     inverse = 10000.0 ** (-jnp.arange(half_size, dtype=jnp.float32) / half_size)
     angles = positions.astype(jnp.float32)[:, None] * inverse[None, :]
-    cosine = jnp.cos(angles)[:, None, :]
-    sine = jnp.sin(angles)[:, None, :]
-    first_half = heads[..., :half_size]
-    second_half = heads[..., half_size:]
-    turned = jnp.concatenate(
-        [first_half * cosine - second_half * sine, second_half * cosine + first_half * sine],
-        axis=-1,
+    cosine, sine = jnp.cos(angles), jnp.sin(angles)
+    cosine = jnp.concatenate([cosine, cosine], axis=1)
+    sine = jnp.concatenate([-sine, sine], axis=1)
+    vmem = pl.BlockSpec(memory_space=pltpu.VMEM)
+    anywhere = pl.BlockSpec(memory_space=pl.ANY)
+    half = jnp.bfloat16
+    wide = tok_rows + 2 * W
+    return pl.pallas_call(
+        functools.partial(attention_kernel, sp_count, tp_count),
+        out_shape=jax.ShapeDtypeStruct((tok_rows // tp_count, width * tp_count), half),
+        in_specs=[vmem, anywhere, anywhere, anywhere, vmem, vmem, vmem,
+                  pl.BlockSpec(memory_space=pltpu.SMEM)],
+        out_specs=vmem,
+        scratch_shapes=[
+            pltpu.VMEM((wide, keys.shape[1]), half),
+            pltpu.VMEM((wide, keys.shape[1]), half),
+            pltpu.VMEM((blocks + 2, 1, W), jnp.int32),
+            pltpu.VMEM((wide, keys.shape[1]), half),
+            pltpu.VMEM((tok_rows, width), half),
+            pltpu.SemaphoreType.DMA((4,)),
+            pltpu.SemaphoreType.DMA((6,)),
+            pltpu.SemaphoreType.DMA((6,)),
+            pltpu.SemaphoreType.DMA((tp_count,)),
+            pltpu.SemaphoreType.DMA((tp_count,)),
+        ],
+        compiler_params=pltpu.CompilerParams(collective_id=1, has_side_effects=True),
+        cost_estimate=pl.CostEstimate(
+            flops=4 * tok_rows * 3 * W * width,
+            bytes_accessed=4 * tok_rows * width,
+            transcendentals=tok_rows * 3 * W * width // HD,
+        ),
+        name="attention",
+    )(
+        queries, keys, values, documents.reshape(blocks, 1, W), documents[:, None],
+        cosine, sine, jnp.exp(sink),
     )
-    return turned.reshape(total, head_count * HD).astype(jnp.bfloat16)
-
-
-def rms_scale(vector):
-    return vector * lax.rsqrt(jnp.mean(vector * vector, axis=-1, keepdims=True) + 1e-06)
-
-
-def windows(padded_rows, blocks):
-    tiled = padded_rows.reshape((blocks + 2, W) + padded_rows.shape[1:])
-    return jnp.concatenate([tiled[:-2], tiled[1:-1], tiled[2:]], axis=1)
 
 
 def flipped(index, bits, size):
@@ -72,6 +216,9 @@
     across = flipped(tp, 2, tp_count)
     SP, ACROSS, NEAR, NEAR2, CORE, BACK, HOME = range(7)
 
+    def bits_of(step):
+        return step // 2 + (step % 2) * (sp_count // 2)
+
     def remote(kind, step, source, target, device):
         return pltpu.make_async_remote_copy(
             src_ref=source,
@@ -83,7 +230,7 @@
         )
 
     def out_copy(step):
-        peer = flipped(me, step, sp_count)
+        peer = flipped(me, bits_of(step), sp_count)
         return remote(SP, step, outgoing.at[peer], rows.at[step, 0], {"sp": peer})
 
     def across_copy(step):
@@ -102,7 +249,7 @@
         return remote(BACK, step, y_out.at[step], y_in.at[step], {"tp": across})
 
     def home_copy(step):
-        peer = flipped(me, step, sp_count)
+        peer = flipped(me, bits_of(step), sp_count)
         return remote(HOME, step, done_out.at[step], returned.at[me], {"sp": peer})
 
     weights = [
@@ -212,7 +359,7 @@
         def _():
             home_copy(step).start()
 
-    stages = ((forward_again, 1), (compute, 2), (add_core, 3), (add_across, 4), (forward, 0))
+    stages = ((forward, 0), (forward_again, 1), (compute, 2), (add_core, 3), (add_across, 4))
 
     def turn(number, carry):
         for stage, lag in stages:
@@ -298,47 +445,9 @@
     up_weight,
     down_weight,
 ):
-    tok_rows = queries.shape[0]
-    head_count = queries.shape[1] // HD
-    kv_count = keys.shape[1] // HD
-    group_size = head_count // kv_count
     sp_count = lax.axis_size("sp")
-    tp_count = lax.axis_size("tp")
-    offset = lax.axis_index("sp") * tok_rows
-    positions = offset + jnp.arange(tok_rows, dtype=jnp.int32)
-    q_turned = turn_heads(queries, positions, head_count)
-    k_turned = turn_heads(keys, positions, kv_count)
-    paired = jnp.concatenate([k_turned, values], axis=1)
-    wide_pairs, wide_docs = (
-        extended(paired, (("sp", 0),), W),
-        extended(documents, (("sp", 0),), W),
-    )
-    blocks = tok_rows // W
-    query_blocks = q_turned.reshape(blocks, W, kv_count, group_size, HD)
-    pair_win = windows(wide_pairs, blocks)
-    key_win = pair_win[..., : kv_count * HD].reshape(blocks, 3 * W, kv_count, HD)
-    value_win = pair_win[..., kv_count * HD :].reshape(blocks, 3 * W, kv_count, HD)
-    doc_win = windows(wide_docs, blocks)
-    doc_query = documents.reshape(blocks, W)
-    block_ids = jnp.arange(blocks, dtype=jnp.int32)[:, None, None]
-    query_pos = offset + block_ids * W + jnp.arange(W, dtype=jnp.int32)[None, :, None]
-    key_pos = offset + (block_ids - 1) * W + jnp.arange(3 * W, dtype=jnp.int32)[None, None, :]
-    keep_mask = (
-        (jnp.abs(query_pos - key_pos) <= W) & (key_pos >= 0) & (key_pos < tok_rows * sp_count)
-    )
-    keep_mask = keep_mask & (doc_query[:, :, None] == doc_win[:, None, :])
-    scores = jnp.einsum(
-        "nqhgd,nkhd->nhgqk", query_blocks, key_win, preferred_element_type=jnp.float32
-    ) * HD ** (-0.5)
-    exponent = jnp.where(keep_mask[:, None, None], jnp.exp(scores), 0.0)
-    denominator = jnp.sum(exponent, axis=-1, keepdims=True) + jnp.exp(sink).reshape(
-        1, kv_count, group_size, 1, 1
-    )
-    probs = (exponent / denominator).astype(jnp.bfloat16)
-    attended = jnp.einsum("nhgqk,nkhd->nqhgd", probs, value_win, preferred_element_type=jnp.float32)
-    attended = attended.astype(jnp.bfloat16).reshape(tok_rows, head_count * HD)
-    own_rows = tok_rows // tp_count
-    all_heads = lax.all_to_all(attended, "tp", split_axis=0, concat_axis=1, tiled=True)
+    own_rows = residual.shape[0]
+    all_heads = run_attention(queries, keys, values, documents, sink)
     projected = jnp.dot(all_heads, out_weight, preferred_element_type=jnp.float32)
     after_mix = residual.astype(jnp.float32) + rms_scale(projected) * mix_gain
     normed = (rms_scale(after_mix) * ffn_gain).astype(jnp.bfloat16)

time: 178 us -> 154 us (0.87)
  the two profiles are of different devices: /device:TPU:18 before, /device:TPU:0 now
where the time goes in v2:
time: 154 us
  Pallas kernels  138 us (90%)
  matrix products  8.39 us (5%)
  other arithmetic  3.88 us (3%)
  local copies, waits for them, and re-layouts  3.6 us (2%)
    pallas_call x1, Pallas kernels, run_experts(): pl.pallas_call(functools.partial(expert_kernel, sp_count, tp_count, capac...  119 us
    pallas_call x1, Pallas kernels, run_attention(): pl.pallas_call(functools.partial(attention_kernel, sp_count, tp_count), o...  18.7 us
    dot_general x1, matrix products, body(): jnp.dot(all_heads, out_weight, preferred_element_type=jnp.float32)  3.24 us

profile of v2, /device:TPU:0, one launch (start us, length us, event | category | flops | bytes accessed | tf_op | source)
XLA Modules:
  0.0 154.1 jit_solution(7952230917565762388)
XLA Ops:
  0.0 1.2 fusion.11
  1.3 1.1 pad_maximum_fusion
  2.3 0.0 copy-done.7
  2.3 0.8 broadcast_in_dim.61.doc_column
  3.1 0.0 copy-done.3
  3.1 0.7 copy.29.keys
  3.8 0.0 copy-done.4
  3.8 0.7 copy.30.values
  4.6 0.6 reshape.80.documents
  5.1 0.0 copy-done.10
  5.1 0.6 exp.6.sink_terms
  5.7 18.7 %attention.1 = bf16[96,1024]{1,0:T(8,128)(2,1)} custom-call(bf16[384,256]{1,0:T(8,128)(2,1)} %queries.1, bf16[384,64]{1,0:T(8,128)(2,1)} %copy.29.keys, bf16[384,64]{1,0:T(8,128)(2,1)} %copy.30.values, s32[3,1,128]{2,1,0:T(1,128)} %reshape.80.documents, s32[384,1]{1,0:T(8,128)} %broadcast_in_dim.61.doc_column, f32[640,64]{1,0:T(8,128)} %get-tuple-element.12.cosine, ...), custom_call_target="tpu_custom_call" | custom-call | flops 150994944 | bytes 393216 | tf_op jit(solution)/shard_map/attention/pallas_call | solution.py:167
  24.4 0.0 copy-start.1
  24.4 0.0 copy-start.2
  24.4 0.0 copy-start.9
  24.5 0.0 copy-start.5
  24.5 3.2 %multiply_reduce_fusion.2 = (f32[96]{0:T(128)S(1)}, f32[96,2048]{1,0:T(8,128)S(1)}) fusion(bf16[96,1024]{1,0:T(8,128)(2,1)} %attention.1, bf16[1024,2048]{1,0:T(8,128)(2,1)} %param.21), kind=kOutput, calls=%fused_computation.12 | convolution fusion | flops 403046304 | bytes 5177728 | tf_op jit(solution)/shard_map/dot_general | solution.py:451
  27.7 0.0 copy-done.1
  27.7 0.0 copy-done.2
  27.8 0.3 multiply_reduce_fusion.1
  28.1 0.0 copy-done.9
  28.1 0.1 fusion.2
  28.2 0.1 eq.59
  28.3 0.2 bitcast_compare_fusion
  28.5 0.0 copy-done.5
  28.5 2.2 %convolution_convert_fusion = bf16[512,2048]{1,0:T(8,128)(2,1)} fusion(pred[512,96]{1,0:T(32,128)(4,1)S(1)} %bitcast_compare_fusion, f32[2048]{0:T(1024)S(1)} %copy-done.5, f32[96]{0:T(128)S(1)} %add_rsqrt_fusion.1, f32[96,2048]{1,0:T(8,128)S(1)} %get-tuple-element.9, bf16[96,2048]{1,0:T(8,128)(2,1)S(1)} %copy-done.1, f32[2048]{0:T(1024)S(1)} %copy-done.2, ...), kind=kOutput, calls=%fused_computation | convolution fusion | flops 203751424 | bytes 3343104 | tf_op jit(solution)/shard_map/dot_general | solution.py:470
  30.7 119.4 %experts.1 = bf16[8,64,2048]{2,1,0:T(8,128)(2,1)} custom-call(bf16[8,64,2048]{2,1,0:T(8,128)(2,1)} %bitcast.16, bf16[1,2048,512]{2,1,0:T(8,128)(2,1)} %gate_hbm.1, bf16[1,2048,512]{2,1,0:T(8,128)(2,1)} %up_hbm.1, bf16[1,512,2048]{2,1,0:T(8,128)(2,1)} %down_hbm.1), custom_call_target="tpu_custom_call" | custom-call | flops 12884901888 | bytes 6291456 | tf_op jit(solution)/shard_map/experts/pallas_call | solution.py:399
  150.1 2.2 %convolution_bitcast_fusion = f32[96,2048]{1,0:T(8,128)S(1)} fusion(bf16[8,64,2048]{2,1,0:T(8,128)(2,1)} %experts.1, bf16[96,8]{0,1:T(8,128)(2,1)S(1)} %fusion.13, s32[96,8]{0,1:T(8,128)S(1)} %fusion.2), kind=kOutput, calls=%fused_computation.1 | convolution fusion | flops 201424896 | bytes 2888192 | tf_op jit(solution)/shard_map/dot_general | solution.py:485
  152.4 0.0 copy-done
  152.4 0.6 multiply_reduce_fusion
  153.0 0.1 copy-done.6
  153.0 1.0 add_convert_fusion
  (20 shorter events, 0.1 us)
Async XLA Ops:
  0.0 2.3 %copy-start.7 = (s32[384]{0:T(512)S(1)}, s32[384]{0:T(512)}, u32[]{:S(2)}) copy-start(s32[384]{0:T(512)} %param.19) | copy-start | bytes 4612
  0.0 3.1 %copy-start.3 = (bf16[384,64]{0,1:T(8,128)(2,1)S(1)}, bf16[384,64]{0,1:T(8,128)(2,1)}, u32[]{:S(2)}) copy-start(bf16[384,64]{0,1:T(8,128)(2,1)} %param.17) | copy-start | bytes 147460
  0.0 3.8 %copy-start.4 = (bf16[384,64]{0,1:T(8,128)(2,1)S(1)}, bf16[384,64]{0,1:T(8,128)(2,1)}, u32[]{:S(2)}) copy-start(bf16[384,64]{0,1:T(8,128)(2,1)} %param.18) | copy-start | bytes 147460
  0.0 5.1 %copy-start.10 = (f32[4]{0:T(128)S(1)}, f32[4]{0:T(128)}, u32[]{:S(2)}) copy-start(f32[4]{0:T(128)} %param.20) | copy-start | bytes 52
  24.4 3.3 %copy-start.1 = (bf16[96,2048]{1,0:T(8,128)(2,1)S(1)}, bf16[96,2048]{1,0:T(8,128)(2,1)}, u32[]{:S(2)}) copy-start(bf16[96,2048]{1,0:T(8,128)(2,1)} %param.15) | copy-start | bytes 1179652
  24.4 3.3 %copy-start.2 = (f32[2048]{0:T(1024)S(1)}, f32[2048]{0:T(1024)}, u32[]{:S(2)}) copy-start(f32[2048]{0:T(1024)} %param.22) | copy-start | bytes 24580
  24.4 3.6 %copy-start.9 = (s32[96,4]{0,1:T(4,128)S(1)}, s32[96,4]{0,1:T(4,128)}, u32[]{:S(2)}) copy-start(s32[96,4]{0,1:T(4,128)} %param.25) | copy-start | bytes 4612
  24.5 4.0 %copy-start.5 = (f32[2048]{0:T(1024)S(1)}, f32[2048]{0:T(1024)}, u32[]{:S(2)}) copy-start(f32[2048]{0:T(1024)} %param.23) | copy-start | bytes 24580
  30.7 119.4 %copy-start.8 = (f32[96,4]{0,1:T(4,128)S(1)}, f32[96,4]{0,1:T(4,128)}, u32[]{:S(2)}) copy-start(f32[96,4]{0,1:T(4,128)} %param.26) | copy-start | bytes 4612
  150.0 2.3 %copy-start = (bf16[8,64,2048]{2,1,0:T(8,128)(2,1)S(1)}, bf16[8,64,2048]{2,1,0:T(8,128)(2,1)}, u32[]{:S(2)}) copy-start(bf16[8,64,2048]{2,1,0:T(8,128)(2,1)} %experts.1) | copy-start | bytes 6291460
  152.3 0.7 copy-start.6

commit v3 on v2

--- a/solution.py
+++ b/solution.py
@@ -10,6 +10,7 @@
 HD = 64
 TOPK = 4
 W = 128
+PIECES = 2
 
 
 def rms_scale(vector):
@@ -216,8 +217,11 @@
     across = flipped(tp, 2, tp_count)
     SP, ACROSS, NEAR, NEAR2, CORE, BACK, HOME = range(7)
 
+    pieces = outgoing.shape[1]
+    steps = sp_count * pieces
+
     def bits_of(step):
-        return step // 2 + (step % 2) * (sp_count // 2)
+        return step // pieces
 
     def remote(kind, step, source, target, device):
         return pltpu.make_async_remote_copy(
@@ -231,7 +235,7 @@
 
     def out_copy(step):
         peer = flipped(me, bits_of(step), sp_count)
-        return remote(SP, step, outgoing.at[peer], rows.at[step, 0], {"sp": peer})
+        return remote(SP, step, outgoing.at[peer, step % pieces], rows.at[step, 0], {"sp": peer})
 
     def across_copy(step):
         return remote(ACROSS, step, rows.at[step, 0], rows.at[step, 1], {"tp": across})
@@ -250,17 +254,25 @@
 
     def home_copy(step):
         peer = flipped(me, bits_of(step), sp_count)
-        return remote(HOME, step, done_out.at[step], returned.at[me], {"sp": peer})
+        return remote(HOME, step, done_out.at[step], returned.at[me, step % pieces], {"sp": peer})
 
     weights = [
         pltpu.make_async_copy(source, target, weight_sem.at[n])
         for n, (source, target) in enumerate(((gate_hbm, gate), (up_hbm, up), (down_hbm, down)))
     ]
-    own_in = pltpu.make_async_copy(outgoing.at[me], rows.at[0, 0], local_sem.at[0])
-    own_out = pltpu.make_async_copy(done_out.at[0], returned.at[me], local_sem.at[1])
+    own_in = [
+        pltpu.make_async_copy(outgoing.at[me, n], rows.at[n, 0], local_sem.at[0, n])
+        for n in range(pieces)
+    ]
+
+    def own_out(step):
+        return pltpu.make_async_copy(
+            done_out.at[step], returned.at[me, step], local_sem.at[1, step]
+        )
 
     barrier = pltpu.get_barrier_semaphore()
-    own_in.start()
+    for copy in own_in:
+        copy.start()
 
     def greet(step, carry):
         pl.semaphore_signal(
@@ -280,17 +292,18 @@
         out_copy(step).start()
         return carry
 
-    lax.fori_loop(1, sp_count, send_out, 0)
+    lax.fori_loop(pieces, steps, send_out, 0)
     for copy in weights:
         copy.start()
-    own_in.wait()
+    for copy in own_in:
+        copy.wait()
 
     local_experts, width, units = gate.shape
     slots = rows.shape[2]
     chunk = tp_count * slots
 
     def forward(step):
-        @pl.when(step > 0)
+        @pl.when(step >= pieces)
         def _():
             out_copy(step).wait_recv()
 
@@ -319,7 +332,8 @@
             hidden = (upper + 1.0) * gated * jax.nn.sigmoid(1.702 * gated)
             if local_experts > 1:
                 row = lax.broadcasted_iota(jnp.int32, (chunk, units), 0)
-                hidden = jnp.where((row // capacity) % local_experts == expert, hidden, 0.0)
+                slot = (step % pieces) * slots + row % slots
+                hidden = jnp.where(slot // capacity == expert, hidden, 0.0)
             hiddens.append(hidden.astype(jnp.bfloat16))
         tile = width // 4
         for start in range(0, width, tile):
@@ -351,11 +365,11 @@
             + y_in[step].astype(jnp.float32)
         ).astype(jnp.bfloat16)
 
-        @pl.when(step == 0)
+        @pl.when(step < pieces)
         def _():
-            own_out.start()
-
-        @pl.when(step > 0)
+            own_out(step).start()
+
+        @pl.when(step >= pieces)
         def _():
             home_copy(step).start()
 
@@ -365,16 +379,16 @@
         for stage, lag in stages:
             step = number - lag
 
-            @pl.when((step >= 0) & (step < sp_count))
+            @pl.when((step >= 0) & (step < steps))
             def _():
                 stage(step)
 
         return carry
 
-    lax.fori_loop(0, sp_count + 4, turn, 0)
+    lax.fori_loop(0, steps + 4, turn, 0)
 
     def finish(step, carry):
-        @pl.when(step > 0)
+        @pl.when(step >= pieces)
         def _():
             out_copy(step).wait_send()
             home_copy(step).wait_send()
@@ -384,16 +398,20 @@
             make(step).wait_send()
         return carry
 
-    lax.fori_loop(0, sp_count, finish, 0)
-    own_out.wait()
+    lax.fori_loop(0, steps, finish, 0)
+    for n in range(pieces):
+        own_out(n).wait()
 
 
 def run_experts(outgoing, gate_weight, up_weight, down_weight, capacity):
     sp_count, slots, width = outgoing.shape
+    pieces = PIECES if slots % (16 * PIECES) == 0 else 1
+    outgoing = outgoing.reshape(sp_count, pieces, slots // pieces, width)
+    steps, slots = sp_count * pieces, slots // pieces
     tp_count = lax.axis_size("tp")
     assert tp_count == 4
     local_experts, _, units = gate_weight.shape
-    rows = sp_count * tp_count * slots
+    rows = steps * tp_count * slots
     half = jnp.bfloat16
     anywhere = pl.BlockSpec(memory_space=pl.ANY)
     return pl.pallas_call(
@@ -405,16 +423,16 @@
             pltpu.VMEM(gate_weight.shape, half),
             pltpu.VMEM(up_weight.shape, half),
             pltpu.VMEM(down_weight.shape, half),
-            pltpu.VMEM((sp_count, tp_count, slots, width), half),
-            pltpu.VMEM((sp_count, tp_count, slots, width), half),
-            pltpu.VMEM((sp_count, 2, slots, width), half),
-            pltpu.VMEM((sp_count, slots, width), half),
-            pltpu.VMEM((sp_count, slots, width), half),
-            pltpu.VMEM((sp_count, slots, width), half),
+            pltpu.VMEM((steps, tp_count, slots, width), half),
+            pltpu.VMEM((steps, tp_count, slots, width), half),
+            pltpu.VMEM((steps, 2, slots, width), half),
+            pltpu.VMEM((steps, slots, width), half),
+            pltpu.VMEM((steps, slots, width), half),
+            pltpu.VMEM((steps, slots, width), half),
             pltpu.SemaphoreType.DMA((3,)),
-            pltpu.SemaphoreType.DMA((2,)),
-            pltpu.SemaphoreType.DMA((7, sp_count)),
-            pltpu.SemaphoreType.DMA((7, sp_count)),
+            pltpu.SemaphoreType.DMA((2, pieces)),
+            pltpu.SemaphoreType.DMA((7, steps)),
+            pltpu.SemaphoreType.DMA((7, steps)),
         ],
         compiler_params=pltpu.CompilerParams(
             collective_id=0, has_side_effects=True, vmem_limit_bytes=60 * 1024 * 1024

time: 154 us -> 146 us (0.948)
  the two profiles are of different devices: /device:TPU:0 before, /device:TPU:18 now
where the time goes in v3:
time: 146 us; the launch traced here: 145 us
  Pallas kernels  129 us (88%)
  matrix products  8.37 us (6%)
  other arithmetic  3.94 us (3%)
  local copies, waits for them, and re-layouts  3.61 us (2%)
    pallas_call x1, Pallas kernels, run_experts(): pl.pallas_call(functools.partial(expert_kernel, sp_count, tp_count, capac...  114 us
    pallas_call x1, Pallas kernels, run_attention(): pl.pallas_call(functools.partial(attention_kernel, sp_count, tp_count), o...  15.3 us
    dot_general x1, matrix products, body(): jnp.dot(all_heads, out_weight, preferred_element_type=jnp.float32)  3.24 us

profile of v3, /device:TPU:18, one launch (start us, length us, event | category | flops | bytes accessed | tf_op | source)
XLA Modules:
  0.0 145.5 jit_solution(11222862289808271758)
XLA Ops:
  0.0 0.0 copy-start.10
  0.1 1.2 fusion.4
  1.3 1.1 pad_maximum_fusion
  2.3 0.0 copy-done.7
  2.3 0.8 broadcast_in_dim.61.doc_column
  3.1 0.0 copy-done.3
  3.1 0.7 copy.30.keys
  3.9 0.7 copy.31.values
  4.6 0.6 reshape.133.documents
  5.2 0.0 copy-done.10
  5.2 0.6 exp.6.sink_terms
  5.8 15.3 %attention.1 = bf16[96,1024]{1,0:T(8,128)(2,1)} custom-call(bf16[384,256]{1,0:T(8,128)(2,1)} %queries.1, bf16[384,64]{1,0:T(8,128)(2,1)} %copy.30.keys, bf16[384,64]{1,0:T(8,128)(2,1)} %copy.31.values, s32[3,1,128]{2,1,0:T(1,128)} %reshape.133.documents, s32[384,1]{1,0:T(8,128)} %broadcast_in_dim.61.doc_column, f32[640,64]{1,0:T(8,128)} %get-tuple-element.14.cosine, ...), custom_call_target="tpu_custom_call" | custom-call | flops 150994944 | bytes 393216 | tf_op jit(solution)/shard_map/attention/pallas_call | solution.py:168
  21.1 0.0 copy-start.1
  21.1 0.0 copy-start.2
  21.1 0.0 copy-start.9
  21.1 0.0 copy-start.5
  21.1 3.2 %multiply_reduce_fusion.2 = (f32[96]{0:T(128)S(1)}, f32[96,2048]{1,0:T(8,128)S(1)}) fusion(bf16[96,1024]{1,0:T(8,128)(2,1)} %attention.1, bf16[1024,2048]{1,0:T(8,128)(2,1)} %param.21), kind=kOutput, calls=%fused_computation.10 | convolution fusion | flops 403046304 | bytes 5177728 | tf_op jit(solution)/shard_map/dot_general | solution.py:469
  24.4 0.0 copy-done.1
  24.4 0.0 copy-done.2
  24.4 0.3 multiply_reduce_fusion.1
  24.7 0.1 fusion.1
  24.9 0.1 eq.71
  24.9 0.2 bitcast_compare_fusion
  25.1 2.2 %convolution_convert_fusion = bf16[512,2048]{1,0:T(8,128)(2,1)} fusion(pred[512,96]{1,0:T(32,128)(4,1)S(1)} %bitcast_compare_fusion, f32[2048]{0:T(1024)S(1)} %copy-done.5, f32[96]{0:T(128)S(1)} %add_rsqrt_fusion.1, f32[96,2048]{1,0:T(8,128)S(1)} %get-tuple-element.11, bf16[96,2048]{1,0:T(8,128)(2,1)S(1)} %copy-done.1, f32[2048]{0:T(1024)S(1)} %copy-done.2, ...), kind=kOutput, calls=%fused_computation | convolution fusion | flops 203751424 | bytes 3343104 | tf_op jit(solution)/shard_map/dot_general | solution.py:488
  27.3 114.1 %experts.1 = bf16[8,2,32,2048]{3,2,1,0:T(8,128)(2,1)} custom-call(bf16[8,2,32,2048]{3,2,1,0:T(8,128)(2,1)} %bitcast.17, bf16[1,2048,512]{2,1,0:T(8,128)(2,1)} %gate_hbm.1, bf16[1,2048,512]{2,1,0:T(8,128)(2,1)} %up_hbm.1, bf16[1,512,2048]{2,1,0:T(8,128)(2,1)} %down_hbm.1), custom_call_target="tpu_custom_call" | custom-call | flops 12884901888 | bytes 6291456 | tf_op jit(solution)/shard_map/experts/pallas_call | solution.py:417
  141.4 0.0 copy-start
  141.4 0.0 copy-done.8
  141.5 0.1 select_convert_fusion
  141.5 2.2 %fusion.7 = f32[96,2048]{1,0:T(8,128)S(1)} fusion(bf16[96,512]{0,1:T(8,128)(2,1)S(1)} %bitcast.19, bf16[512,2048]{1,0:T(8,128)(2,1)} %bitcast.15), kind=kOutput, calls=%fused_computation.35 | convolution fusion | flops 201326592 | bytes 2981888 | tf_op jit(solution)/shard_map/dot_general | solution.py:502
  143.8 0.6 multiply_reduce_fusion
  144.4 0.1 copy-done.6
  144.5 1.0 add_convert_fusion
  (21 shorter events, 0.1 us)
Async XLA Ops:
  0.0 2.3 %copy-start.7 = (s32[384]{0:T(512)S(1)}, s32[384]{0:T(512)}, u32[]{:S(2)}) copy-start(s32[384]{0:T(512)} %param.19) | copy-start | bytes 4612
  0.0 3.1 %copy-start.3 = (bf16[384,64]{0,1:T(8,128)(2,1)S(1)}, bf16[384,64]{0,1:T(8,128)(2,1)}, u32[]{:S(2)}) copy-start(bf16[384,64]{0,1:T(8,128)(2,1)} %param.17) | copy-start | bytes 147460
  0.0 3.9 %copy-start.4 = (bf16[384,64]{0,1:T(8,128)(2,1)S(1)}, bf16[384,64]{0,1:T(8,128)(2,1)}, u32[]{:S(2)}) copy-start(bf16[384,64]{0,1:T(8,128)(2,1)} %param.18) | copy-start | bytes 147460
  0.0 5.2 %copy-start.10 = (f32[4]{0:T(128)S(1)}, f32[4]{0:T(128)}, u32[]{:S(2)}) copy-start(f32[4]{0:T(128)} %param.20) | copy-start | bytes 52
  21.1 3.3 %copy-start.1 = (bf16[96,2048]{1,0:T(8,128)(2,1)S(1)}, bf16[96,2048]{1,0:T(8,128)(2,1)}, u32[]{:S(2)}) copy-start(bf16[96,2048]{1,0:T(8,128)(2,1)} %param.15) | copy-start | bytes 1179652
  21.1 3.3 %copy-start.2 = (f32[2048]{0:T(1024)S(1)}, f32[2048]{0:T(1024)}, u32[]{:S(2)}) copy-start(f32[2048]{0:T(1024)} %param.22) | copy-start | bytes 24580
  21.1 3.6 %copy-start.9 = (s32[96,4]{0,1:T(4,128)S(1)}, s32[96,4]{0,1:T(4,128)}, u32[]{:S(2)}) copy-start(s32[96,4]{0,1:T(4,128)} %param.25) | copy-start | bytes 4612
  21.1 4.0 %copy-start.5 = (f32[2048]{0:T(1024)S(1)}, f32[2048]{0:T(1024)}, u32[]{:S(2)}) copy-start(f32[2048]{0:T(1024)} %param.23) | copy-start | bytes 24580
  27.3 114.1 %copy-start.8 = (f32[96,4]{0,1:T(4,128)S(1)}, f32[96,4]{0,1:T(4,128)}, u32[]{:S(2)}) copy-start(f32[96,4]{0,1:T(4,128)} %param.26) | copy-start | bytes 4612
  141.4 2.4 %copy-start = (bf16[8,2,32,2048]{3,2,1,0:T(8,128)(2,1)S(1)}, bf16[8,2,32,2048]{3,2,1,0:T(8,128)(2,1)}, u32[]{:S(2)}) copy-start(bf16[8,2,32,2048]{3,2,1,0:T(8,128)(2,1)} %experts.1) | copy-start | bytes 6291460
  143.8 0.7 copy-start.6

commit v4 on v3

--- a/solution.py
+++ b/solution.py
@@ -19,9 +19,9 @@
 
 def attention_kernel(
     sp_count, tp_count,
-    queries, keys, values, documents, doc_column, cosine, sine, sink_terms,
+    queries, paired, documents, doc_column, cosine, sine, sink_logits,
     heads_out,
-    wide_keys, wide_values, wide_docs, turned_keys, attended,
+    wide_pairs, wide_docs, turned_keys, attended,
     local_sem, send_sem, recv_sem, out_send, out_recv,
 ):
     me = lax.axis_index("sp")
@@ -30,7 +30,8 @@
     left = (me + sp_count - 1) % sp_count
     tok_rows, width = queries.shape
     blocks = tok_rows // W
-    kv_count = keys.shape[1] // HD
+    kv_width = paired.shape[1] // 2
+    kv_count = kv_width // HD
     group_size = width // HD // kv_count
     own_rows = tok_rows // tp_count
     total = tok_rows * sp_count
@@ -41,8 +42,7 @@
         pltpu.make_async_copy(source, target, local_sem.at[n])
         for n, (source, target) in enumerate(
             (
-                (keys, wide_keys.at[inside]),
-                (values, wide_values.at[inside]),
+                (paired, wide_pairs.at[inside]),
                 (documents, wide_docs.at[pl.ds(1, blocks)]),
             )
         )
@@ -62,11 +62,9 @@
     low, high = pl.ds(0, W), pl.ds(tok_rows + W, W)
     last = pl.ds(tok_rows - W, W)
     pairs = (
-        (keys.at[last], wide_keys.at[low], right),
-        (values.at[last], wide_values.at[low], right),
+        (paired.at[last], wide_pairs.at[low], right),
         (documents.at[blocks - 1], wide_docs.at[0], right),
-        (keys.at[low], wide_keys.at[high], left),
-        (values.at[low], wide_values.at[high], left),
+        (paired.at[low], wide_pairs.at[high], left),
         (documents.at[0], wide_docs.at[blocks + 1], left),
     )
     halos = [
@@ -101,7 +99,7 @@
         copy.wait()
     for n in range(blocks + 2):
         rows = slice(n * W, (n + 1) * W)
-        turned_keys[rows, :] = turn(wide_keys[rows, :], rows)
+        turned_keys[rows, :] = turn(wide_pairs[rows, :kv_width], rows)
 
     scale = HD ** (-0.5)
     for n in range(blocks):
@@ -121,9 +119,11 @@
                 (((1,), (1,)), ((), ())), preferred_element_type=jnp.float32,
             ) * scale
             exponent = jnp.where(keep, jnp.exp(scores), 0.0)
-            denominator = jnp.sum(exponent, axis=-1, keepdims=True) + sink_terms[head]
+            sink_term = jnp.exp(jnp.full((W, 1), sink_logits[head], jnp.float32))
+            denominator = jnp.sum(exponent, axis=-1, keepdims=True) + sink_term
             probs = (exponent / denominator).astype(jnp.bfloat16)
-            found = jnp.dot(probs, wide_values[window, kv], preferred_element_type=jnp.float32)
+            held = slice(kv_width + kv.start, kv_width + kv.stop)
+            found = jnp.dot(probs, wide_pairs[window, held], preferred_element_type=jnp.float32)
             attended[n * W : (n + 1) * W, columns] = found.astype(jnp.bfloat16)
 
     def share(index):
@@ -168,18 +168,17 @@
     return pl.pallas_call(
         functools.partial(attention_kernel, sp_count, tp_count),
         out_shape=jax.ShapeDtypeStruct((tok_rows // tp_count, width * tp_count), half),
-        in_specs=[vmem, anywhere, anywhere, anywhere, vmem, vmem, vmem,
+        in_specs=[vmem, anywhere, anywhere, vmem, vmem, vmem,
                   pl.BlockSpec(memory_space=pltpu.SMEM)],
         out_specs=vmem,
         scratch_shapes=[
-            pltpu.VMEM((wide, keys.shape[1]), half),
-            pltpu.VMEM((wide, keys.shape[1]), half),
+            pltpu.VMEM((wide, 2 * keys.shape[1]), half),
             pltpu.VMEM((blocks + 2, 1, W), jnp.int32),
             pltpu.VMEM((wide, keys.shape[1]), half),
             pltpu.VMEM((tok_rows, width), half),
             pltpu.SemaphoreType.DMA((4,)),
-            pltpu.SemaphoreType.DMA((6,)),
-            pltpu.SemaphoreType.DMA((6,)),
+            pltpu.SemaphoreType.DMA((4,)),
+            pltpu.SemaphoreType.DMA((4,)),
             pltpu.SemaphoreType.DMA((tp_count,)),
             pltpu.SemaphoreType.DMA((tp_count,)),
         ],
@@ -191,8 +190,8 @@
         ),
         name="attention",
     )(
-        queries, keys, values, documents.reshape(blocks, 1, W), documents[:, None],
-        cosine, sine, jnp.exp(sink),
+        queries, jnp.concatenate([keys, values], axis=1), documents.reshape(blocks, 1, W),
+        documents[:, None], cosine, sine, sink,
     )
 
 
@@ -373,7 +372,7 @@
         def _():
             home_copy(step).start()
 
-    stages = ((forward, 0), (forward_again, 1), (compute, 2), (add_core, 3), (add_across, 4))
+    stages = ((forward, 0), (forward_again, 1), (add_core, 3), (add_across, 4), (compute, 2))
 
     def turn(number, carry):
         for stage, lag in stages:

time: 146 us -> 145 us (level)
  local copies, waits for them, and re-layouts: 3.61 us -> 1.82 us
where the time goes in v4:
time: 145 us; the launch traced here: 144 us
  Pallas kernels  129 us (89%)
  matrix products  8.37 us (6%)
  other arithmetic  4.67 us (3%)
  local copies, waits for them, and re-layouts  1.82 us (1%)
    pallas_call x1, Pallas kernels, run_experts(): pl.pallas_call(functools.partial(expert_kernel, sp_count, tp_count, capac...  114 us
    pallas_call x1, Pallas kernels, run_attention(): pl.pallas_call(functools.partial(attention_kernel, sp_count, tp_count), o...  14.9 us
    dot_general x1, matrix products, body(): jnp.dot(all_heads, out_weight, preferred_element_type=jnp.float32)  3.24 us

profile of v4, /device:TPU:18, one launch (start us, length us, event | category | flops | bytes accessed | tf_op | source)
XLA Modules:
  0.0 144.3 jit_solution(5321199527664491924)
XLA Ops:
  0.0 1.2 fusion.4
  1.3 1.1 pad_maximum_fusion
  2.3 0.0 copy-done.3
  2.3 0.1 copy.29
  2.5 0.0 copy-done.4
  2.5 0.1 copy.30
  2.6 0.7 pad_maximum_fusion.2.paired
  3.3 0.0 copy-done.7
  3.3 0.8 broadcast_in_dim.61.doc_column
  4.1 0.6 reshape.133.documents
  4.7 14.9 %attention.1 = bf16[96,1024]{1,0:T(8,128)(2,1)} custom-call(bf16[384,256]{1,0:T(8,128)(2,1)} %queries.1, bf16[384,128]{1,0:T(8,128)(2,1)} %pad_maximum_fusion.2.paired, s32[3,1,128]{2,1,0:T(1,128)} %reshape.133.documents, s32[384,1]{1,0:T(8,128)} %broadcast_in_dim.61.doc_column, f32[640,64]{1,0:T(8,128)} %get-tuple-element.14.cosine, ...), custom_call_target="tpu_custom_call" | custom-call | flops 150994944 | bytes 393216 | tf_op jit(solution)/shard_map/attention/pallas_call | solution.py:168
  19.6 0.0 copy-start.1
  19.6 0.0 copy-start.2
  19.6 0.0 copy-start.9
  19.6 0.0 copy-start.5
  19.6 3.2 %multiply_reduce_fusion.2 = (f32[96]{0:T(128)S(1)}, f32[96,2048]{1,0:T(8,128)S(1)}) fusion(bf16[96,1024]{1,0:T(8,128)(2,1)} %attention.1, bf16[1024,2048]{1,0:T(8,128)(2,1)} %param.21), kind=kOutput, calls=%fused_computation.10 | convolution fusion | flops 403046304 | bytes 5177728 | tf_op jit(solution)/shard_map/dot_general | solution.py:468
  22.9 0.0 copy-done.1
  22.9 0.0 copy-done.2
  22.9 0.3 multiply_reduce_fusion.1
  23.2 0.0 copy-done.9
  23.2 0.1 fusion.1
  23.4 0.1 eq.71
  23.5 0.2 bitcast_compare_fusion
  23.6 0.0 copy-done.5
  23.6 2.2 %convolution_convert_fusion = bf16[512,2048]{1,0:T(8,128)(2,1)} fusion(pred[512,96]{1,0:T(32,128)(4,1)S(1)} %bitcast_compare_fusion, f32[2048]{0:T(1024)S(1)} %copy-done.5, f32[96]{0:T(128)S(1)} %add_rsqrt_fusion.1, f32[96,2048]{1,0:T(8,128)S(1)} %get-tuple-element.11, bf16[96,2048]{1,0:T(8,128)(2,1)S(1)} %copy-done.1, f32[2048]{0:T(1024)S(1)} %copy-done.2, ...), kind=kOutput, calls=%fused_computation | convolution fusion | flops 203751424 | bytes 3343104 | tf_op jit(solution)/shard_map/dot_general | solution.py:487
  25.8 114.4 %experts.1 = bf16[8,2,32,2048]{3,2,1,0:T(8,128)(2,1)} custom-call(bf16[8,2,32,2048]{3,2,1,0:T(8,128)(2,1)} %bitcast.17, bf16[1,2048,512]{2,1,0:T(8,128)(2,1)} %gate_hbm.1, bf16[1,2048,512]{2,1,0:T(8,128)(2,1)} %up_hbm.1, bf16[1,512,2048]{2,1,0:T(8,128)(2,1)} %down_hbm.1), custom_call_target="tpu_custom_call" | custom-call | flops 12884901888 | bytes 6291456 | tf_op jit(solution)/shard_map/experts/pallas_call | solution.py:416
  140.2 0.0 copy-start
  140.3 0.1 select_convert_fusion
  140.4 2.2 %fusion.7 = f32[96,2048]{1,0:T(8,128)S(1)} fusion(bf16[96,512]{0,1:T(8,128)(2,1)S(1)} %bitcast.19, bf16[512,2048]{1,0:T(8,128)(2,1)} %bitcast.15), kind=kOutput, calls=%fused_computation.36 | convolution fusion | flops 201326592 | bytes 2981888 | tf_op jit(solution)/shard_map/dot_general | solution.py:501
  142.6 0.6 multiply_reduce_fusion
  143.2 0.1 copy-done.6
  143.3 1.0 add_convert_fusion
  (19 shorter events, 0.1 us)
Async XLA Ops:
  0.0 2.3 %copy-start.3 = (bf16[384,64]{0,1:T(8,128)(2,1)S(1)}, bf16[384,64]{0,1:T(8,128)(2,1)}, u32[]{:S(2)}) copy-start(bf16[384,64]{0,1:T(8,128)(2,1)} %param.17) | copy-start | bytes 147460
  0.0 2.5 %copy-start.4 = (bf16[384,64]{0,1:T(8,128)(2,1)S(1)}, bf16[384,64]{0,1:T(8,128)(2,1)}, u32[]{:S(2)}) copy-start(bf16[384,64]{0,1:T(8,128)(2,1)} %param.18) | copy-start | bytes 147460
  0.0 3.3 %copy-start.7 = (s32[384]{0:T(512)S(1)}, s32[384]{0:T(512)}, u32[]{:S(2)}) copy-start(s32[384]{0:T(512)} %param.19) | copy-start | bytes 4612
  19.6 3.3 %copy-start.1 = (bf16[96,2048]{1,0:T(8,128)(2,1)S(1)}, bf16[96,2048]{1,0:T(8,128)(2,1)}, u32[]{:S(2)}) copy-start(bf16[96,2048]{1,0:T(8,128)(2,1)} %param.15) | copy-start | bytes 1179652
  19.6 3.3 %copy-start.2 = (f32[2048]{0:T(1024)S(1)}, f32[2048]{0:T(1024)}, u32[]{:S(2)}) copy-start(f32[2048]{0:T(1024)} %param.22) | copy-start | bytes 24580
  19.6 3.6 %copy-start.9 = (s32[96,4]{0,1:T(4,128)S(1)}, s32[96,4]{0,1:T(4,128)}, u32[]{:S(2)}) copy-start(s32[96,4]{0,1:T(4,128)} %param.25) | copy-start | bytes 4612
  19.6 4.0 %copy-start.5 = (f32[2048]{0:T(1024)S(1)}, f32[2048]{0:T(1024)}, u32[]{:S(2)}) copy-start(f32[2048]{0:T(1024)} %param.23) | copy-start | bytes 24580
  25.8 114.4 %copy-start.8 = (f32[96,4]{0,1:T(4,128)S(1)}, f32[96,4]{0,1:T(4,128)}, u32[]{:S(2)}) copy-start(f32[96,4]{0,1:T(4,128)} %param.26) | copy-start | bytes 4612
  140.2 2.4 %copy-start = (bf16[8,2,32,2048]{3,2,1,0:T(8,128)(2,1)S(1)}, bf16[8,2,32,2048]{3,2,1,0:T(8,128)(2,1)}, u32[]{:S(2)}) copy-start(bf16[8,2,32,2048]{3,2,1,0:T(8,128)(2,1)} %experts.1) | copy-start | bytes 6291460
  142.6 0.7 copy-start.6
